TPU v7x, 256 devices: a whole 4x4x8 slice. The times are simulated.
256 devices in a mesh: gr: 2 (over z_hi), fs: 16 (over z_lo, y), tp: 8 (over x, core).
Axes of the slice: x: 4, y: 4, z: 8 (z_hi: 2, z_lo: 4; z = z_hi * 4 + z_lo), core: 2. Of those that a mesh axis runs over, the one named last changes fastest.
Arguments:
- tokens: bfloat16 [8192, 2048], P(('gr', 'fs')), may hold values from -6 to 6
- route_ids: int32 [8192, 4], P(('gr', 'fs')), may hold values from 0 to 15, all different within a row; in each aligned block of 256 rows (0 to 255, 256 to 511, ...) at most 80 rows name the same one
- route_scores: float32 [8192, 4], P(('gr', 'fs')), may hold values from -4 to 4
- norm_gain: float32 [2048], P(('gr', 'fs')), may hold values from 0.1 to 1.9
- gate_weight: float32 [16, 2048, 2048], P(None, ('gr', 'fs'), 'tp'), may hold values from -0.5 to 0.5
- up_weight: float32 [16, 2048, 2048], P(None, ('gr', 'fs'), 'tp'), may hold values from -0.5 to 0.5
- down_weight: float32 [16, 2048, 2048], P(None, ('gr', 'fs'), 'tp'), may hold values from -0.03125 to 0.03125
Outputs:
- served_gate: bfloat16 [16, 2048, 2048], P('fs', None, 'tp')
- served_up: bfloat16 [16, 2048, 2048], P('fs', None, 'tp')
- served_down: bfloat16 [16, 2048, 2048], P('fs', None, 'tp')
- expert_mix: bfloat16 [8192, 2048], P(('gr', 'fs'), 'tp')
Inputs may be any that keep to these rules, and one draw needn't show every extreme that they name: `route_ids`: in each aligned block of 256 rows no expert is named by more than 80 pairs, and in some blocks one expert is named by exactly 80. The 4 experts of a token differ.
All inputs are finite; a program needn't handle non-finite values.
Results may differ from a plain program's by a relative error of at most 0.0092.
Values may be sent and summed in bfloat16 or wider, within the bound.
A program may use at most 64 MiB of HBM per device.

v0:
```python
import jax
import jax.numpy as jnp
from jax import lax
from jax.sharding import PartitionSpec as P

EXPERTS = 16
CAP = 80


norm_eps = 1e-06
clamp_limit = 7.0
sigmoid_slope = 1.702


def sent_together(arrays, axis, split_dim, concat_dim, along):
    ends, at = ([], 0)
    for a in arrays[:-1]:
        at += a.shape[along]
        ends.append(at)
    both = jnp.concatenate(arrays, axis=along)
    return tuple(
        jnp.split(
            lax.all_to_all(both, axis, split_axis=split_dim, concat_axis=concat_dim, tiled=True),
            ends,
            axis=along,
        )
    )


def laid_out(parts, dim):
    lengths = list(parts.shape[1:])
    lengths[dim] *= parts.shape[0]
    return jnp.moveaxis(parts, 0, dim).reshape(lengths)


def from_everyone(array, axis):
    devices = lax.axis_size(axis)
    return lax.all_to_all(
        jnp.broadcast_to(array[None], (devices, *array.shape)), axis, 0, 0, tiled=True
    )


def gathered_copies(array, axis, dim):
    return laid_out(from_everyone(array, axis), dim)


def side_by_side(arrays, axis, dim, along):
    widths = [a.shape[along] for a in arrays]
    both = jnp.concatenate(arrays, axis=along)
    filled = gathered_copies(both, axis, dim)
    return tuple(jnp.split(filled, [sum(widths[:k]) for k in range(1, len(widths))], axis=along))


def route_tables(block_ids, block_scores):
    row_count, top_count = block_ids.shape
    flattened = block_ids.reshape(-1)
    onehot = (flattened[:, None] == jnp.arange(EXPERTS, dtype=jnp.int32)[None, :]).astype(jnp.int32)
    before = jnp.cumsum(onehot, axis=0) - onehot
    slot_index = jnp.sum(before * onehot, axis=1)
    target = flattened * CAP + slot_index
    matches = (target[:, None] == jnp.arange(EXPERTS * CAP, dtype=jnp.int32)[None, :]).astype(
        jnp.float32
    )
    matches = matches.reshape(row_count, top_count, EXPERTS * CAP)
    exponent = jnp.exp(block_scores)
    weights = (exponent / jnp.sum(exponent, axis=1, keepdims=True)).astype(jnp.bfloat16)
    dispatch = jnp.sum(matches, axis=1).T.astype(jnp.bfloat16)
    combine = jnp.einsum("tk,tkc->tc", weights.astype(jnp.float32), matches).astype(jnp.bfloat16)
    return (dispatch, combine)


def activate(gate_pre, up_pre):
    clipped_gate = jnp.minimum(gate_pre, clamp_limit)
    clipped_up = jnp.clip(up_pre, -clamp_limit, clamp_limit)
    return (
        clipped_gate * jax.nn.sigmoid(sigmoid_slope * clipped_gate) * (clipped_up + 1.0)
    ).astype(jnp.bfloat16)


def local(tokens, route_ids, route_scores, norm_gain, gate_weight, up_weight, down_weight):
    scaling = norm_gain[None, :, None]
    folded = (
        (scaling * gate_weight).astype(jnp.bfloat16),
        (scaling * up_weight).astype(jnp.bfloat16),
        down_weight.astype(jnp.bfloat16),
    )
    by_expert = sent_together((folded[0], folded[1], folded[2]), "fs", 0, 1, 2)
    served_gate, served_up, served_down = side_by_side(
        (by_expert[0], by_expert[1], by_expert[2]), "gr", 1, 0
    )
    as_float = tokens.astype(jnp.float32)
    normed = (
        as_float * lax.rsqrt(jnp.mean(as_float * as_float, axis=1, keepdims=True) + norm_eps)
    ).astype(jnp.bfloat16)
    dispatch, combine = route_tables(route_ids, route_scores)
    column_width = normed.shape[1] // lax.axis_size("tp")
    normed = lax.dynamic_slice_in_dim(normed, lax.axis_index("tp") * column_width, column_width, 1)
    slot_rows = jnp.dot(dispatch, normed, preferred_element_type=jnp.float32).astype(jnp.bfloat16)
    outgoing = slot_rows.reshape(EXPERTS, 1, CAP, slot_rows.shape[1])
    portion = lax.all_gather(
        lax.all_to_all(outgoing, "fs", split_axis=0, concat_axis=1, tiled=True),
        "tp",
        axis=3,
        tiled=True,
    )
    gate_pre = jnp.einsum(
        "egnd,edf->egnf", portion, served_gate, preferred_element_type=jnp.float32
    )
    up_pre = jnp.einsum("egnd,edf->egnf", portion, served_up, preferred_element_type=jnp.float32)
    hidden = activate(gate_pre, up_pre)
    summed = jnp.einsum(
        "egnf,efd->egnd",
        lax.all_gather(hidden, "tp", axis=3, tiled=True),
        served_down,
        preferred_element_type=jnp.float32,
    )
    results = summed.astype(jnp.bfloat16)
    returned = lax.all_to_all(results, "fs", split_axis=1, concat_axis=0, tiled=True)
    flattened = returned.reshape(EXPERTS * CAP, returned.shape[3])
    expert_mix = jnp.dot(combine, flattened, preferred_element_type=jnp.float32).astype(
        jnp.bfloat16
    )
    return (served_gate, served_up, served_down, expert_mix)


def solution(mesh):
    in_specs = (
        P(("gr", "fs"), None),
        P(("gr", "fs"), None),
        P(("gr", "fs"), None),
        P(("gr", "fs")),
        P(None, ("gr", "fs"), "tp"),
        P(None, ("gr", "fs"), "tp"),
        P(None, ("gr", "fs"), "tp"),
    )
    out_specs = (
        P("fs", None, "tp"),
        P("fs", None, "tp"),
        P("fs", None, "tp"),
        P(("gr", "fs"), "tp"),
    )
    return jax.shard_map(local, mesh=mesh, in_specs=in_specs, out_specs=out_specs, check_vma=False)
```

profile of v0, /device:TPU:4, one launch (start us, length us, event | category | flops | bytes accessed | tf_op | source)
XLA Modules:
  0.0 249.9 jit_solution(6966143844637540849)
XLA Ops:
  7.2 0.8 copy.39
  8.0 0.1 eq.44
  8.2 0.1 eq.40
  8.3 1.5 convert_element_type.64
  9.9 0.3 multiply_reduce_fusion
  10.2 4.5 %reduce-window.6 = s32[16,8,128]{2,1,0:T(8,128)S(1)} reduce-window(s32[16,8,128]{2,1,0:T(8,128)S(1)} %fusion.29, s32[]{:T(128)} %constant.14.clone.1), window={size=1x1x128 pad=0_0x0_0x127_0}, to_apply=%region_1.0 | reduce-window | flops 2080768 | bytes 131076 | tf_op jit(solution)/shard_map/reduce-window
  14.7 0.1 slice.11
  14.8 0.1 copy.41
  15.0 0.1 broadcast_add_fusion
  15.1 0.1 reduce_sum.40
  15.3 0.1 copy.43
  15.4 0.8 convert_reduce_fusion
  16.2 0.4 convolution_convert_fusion
  16.6 27.9 %all_to_all.38 = bf16[16,1,80,256]{3,2,1,0:T(8,128)(2,1)} all-to-all(bf16[16,1,80,256]{3,2,1,0:T(8,128)(2,1)S(1)} %bitcast.70), channel_id=1, replica_groups=mesh['gr'=2,'fs'=16,'tp'=8] {'fs'}, dimensions={0} | all-to-all | bytes 1310720 | tf_op jit(solution)/shard_map/all_to_all | solution.py:101
  44.7 0.3 multiply_convert_fusion.1
  45.0 0.1 pad_maximum_fusion
  45.2 41.3 %all_to_all.39 = bf16[16,64,768]{2,1,0:T(8,128)(2,1)S(1)} all-to-all(bf16[16,64,768]{2,1,0:T(8,128)(2,1)S(1)} %pad_maximum_fusion), channel_id=1, replica_groups=mesh['gr'=2,'fs'=16,'tp'=8] {'fs'}, dimensions={0} | all-to-all | bytes 3145728 | tf_op jit(solution)/shard_map/all_to_all | solution.py:23
  86.5 0.1 fusion.33
  86.6 0.2 pad_maximum_fusion.1
  86.7 0.2 broadcast_in_dim.2
  87.0 77.2 %all_to_all.40 = bf16[2,3,1024,256]{3,2,1,0:T(8,128)(2,1)S(1)} all-to-all(bf16[2,3,1024,256]{3,2,1,0:T(8,128)(2,1)S(1)} %broadcast_in_dim.2), channel_id=1, replica_groups=mesh['gr'=2,'fs'=16,'tp'=8] {'gr'}, dimensions={0} | all-to-all | bytes 6291456 | tf_op jit(solution)/shard_map/all_to_all | solution.py:38
  164.2 0.2 fusion.32
  164.5 5.2 %fusion.9 = f32[16,80,256]{2,1,0:T(8,128)S(1)} fusion(bf16[2048,256,1]{1,0,2:T(8,128)(2,1)S(1)} %bitcast.76, bf16[16,1,80,2048]{3,2,0,1:T(8,128)(2,1)} %all-gather.5.cloned.1.call-done), kind=kOutput, calls=%fused_computation.13 | convolution fusion | flops 1342504960 | bytes 7602176 | tf_op jit(solution)/shard_map/egnd,edf->egnf/dot_general | solution.py:106
  169.7 2.7 %fusion.18 = bf16[16,80,256]{2,1,0:T(8,128)(2,1)} fusion(bf16[2048,256,1]{1,0,2:T(8,128)(2,1)S(1)} %bitcast.74, bf16[16,1,80,2048]{3,2,0,1:T(8,128)(2,1)S(1)} %copy-done.10, f32[16,80,256]{2,1,0:T(8,128)S(1)} %fusion.9), kind=kOutput, calls=%fused_computation.16 | convolution fusion | flops 1345126400 | bytes 8257536 | tf_op jit(solution)/shard_map/egnd,edf->egnf/dot_general | solution.py:109
  172.4 39.3 %all-gather.7.cloned.1.call-done = bf16[16,80,2048]{2,1,0:T(8,128)(2,1)} async-done(((bf16[16,80,256]{2,1,0:T(8,128)(2,1)}), bf16[16,80,2048]{2,1,0:T(8,128)(2,1)}) %all-gather.7.cloned.1.call-update) | async-done | bytes 5242896 | tf_op jit(solution)/shard_map/all_gather | solution.py:113
  211.7 4.9 %fusion.21 = bf16[1,16,80,256]{3,2,0,1:T(8,128)(2,1)} fusion(bf16[16,80,2048]{2,1,0:T(8,128)(2,1)} %all-gather.7.cloned.1.call-done, bf16[2048,256,1]{1,0,2:T(8,128)(2,1)S(1)} %bitcast.72), kind=kOutput, calls=%fused_computation.19 | convolution fusion | flops 1342504960 | bytes 6946816 | tf_op jit(solution)/shard_map/egnf,efd->egnd/dot_general | solution.py:111
  216.6 7.4 %all-to-all-start.3 = ((bf16[1,16,80,256]{3,2,0,1:T(8,128)(2,1)}), bf16[1,16,80,256]{3,2,0,1:T(8,128)(2,1)S(1)}, u32[]{:S(2)}, u32[]{:S(2)}) async-start(bf16[1,16,80,256]{3,2,0,1:T(8,128)(2,1)} %fusion.21), calls=%async_computation.3 | async-start | bytes 1310720 | tf_op jit(solution)/shard_map/all_to_all | solution.py:118
  224.1 0.2 copy.47
  224.2 0.8 iota_compare_fusion
  225.0 3.4 %fusion.4 = bf16[256,1,1280]{2,1,0:T(2,128)(2,1)S(1)} fusion(bf16[256,4,1]{1,2,0:T(2,128)(2,1)S(1)} %copy.47, pred[256,4,1280]{2,0,1:T(32,128)(4,1)S(1)} %iota_compare_fusion), kind=kOutput, calls=%fused_computation.6 | convolution fusion | flops 2621440 | bytes 1968128 | tf_op jit(solution)/shard_map/tk,tkc->tc/dot_general | solution.py:68
  228.4 13.6 %all-to-all-done.3 = bf16[1,16,80,256]{3,2,0,1:T(8,128)(2,1)S(1)} async-done(((bf16[1,16,80,256]{3,2,0,1:T(8,128)(2,1)}), bf16[1,16,80,256]{3,2,0,1:T(8,128)(2,1)S(1)}, u32[]{:S(2)}, u32[]{:S(2)}) %all-to-all-start.3) | async-done | bytes 655392 | tf_op jit(solution)/shard_map/all_to_all | solution.py:118
  242.1 1.0 convolution_convert_fusion.2
  (37 shorter events, 0.4 us)
Async XLA Ops:
  7.2 157.3 %all-gather.5.cloned.1.call-start = ((), (), s32[]{:S(2)}) async-start(), calls=%async_computation.4 | async-start | bytes 5898240 | tf_op jit(solution)/shard_map/all_gather | solution.py:100
  8.3 1.6 copy-start
  9.9 5.5 %copy-start.7 = (s32[256,4]{0,1:T(4,128)S(1)}, s32[256,4]{0,1:T(4,128)}, u32[]{:S(2)}) copy-start(s32[256,4]{0,1:T(4,128)} %param.8) | copy-start | bytes 12292
  16.6 28.0 %copy-start.1 = (f32[16,64,256]{2,1,0:T(8,128)S(1)}, f32[16,64,256]{2,1,0:T(8,128)}, u32[]{:S(2)}) copy-start(f32[16,64,256]{2,1,0:T(8,128)} %param.13) | copy-start | bytes 3145732
  16.6 28.1 %copy-start.2 = (f32[16,64,256]{2,1,0:T(8,128)S(1)}, f32[16,64,256]{2,1,0:T(8,128)}, u32[]{:S(2)}) copy-start(f32[16,64,256]{2,1,0:T(8,128)} %param.11) | copy-start | bytes 3145732
  16.6 28.1 %copy-start.3 = (f32[16,64,256]{2,1,0:T(8,128)S(1)}, f32[16,64,256]{2,1,0:T(8,128)}, u32[]{:S(2)}) copy-start(f32[16,64,256]{2,1,0:T(8,128)} %param.12) | copy-start | bytes 3145732
  16.6 28.1 %copy-start.9 = (f32[64]{0:T(128)S(1)}, f32[64]{0:T(128)}, u32[]{:S(2)}) copy-start(f32[64]{0:T(128)} %param.10) | copy-start | bytes 772
  44.6 167.1 %all-gather.7.cloned.1.call-start = ((), (), s32[]{:S(2)}) async-start(), calls=%async_computation.5 | async-start | bytes 5898240 | tf_op jit(solution)/shard_map/all_gather | solution.py:113
  164.4 5.3 %copy-start.6 = (bf16[1,2,1024,256]{3,2,0,1:T(8,128)(2,1)}, bf16[1,2,1024,256]{3,2,0,1:T(8,128)(2,1)S(1)}, u32[]{:S(2)}) copy-start(bf16[1,2,1024,256]{3,2,0,1:T(8,128)(2,1)S(1)} %get-tuple-element.6) | copy-start | bytes 3145732
  164.4 5.3 %copy-start.5 = (bf16[1,2,1024,256]{3,2,0,1:T(8,128)(2,1)}, bf16[1,2,1024,256]{3,2,0,1:T(8,128)(2,1)S(1)}, u32[]{:S(2)}) copy-start(bf16[1,2,1024,256]{3,2,0,1:T(8,128)(2,1)S(1)} %get-tuple-element.5) | copy-start | bytes 3145732
  164.4 47.3 %copy-start.4 = (bf16[1,2,1024,256]{3,2,0,1:T(8,128)(2,1)}, bf16[1,2,1024,256]{3,2,0,1:T(8,128)(2,1)S(1)}, u32[]{:S(2)}) copy-start(bf16[1,2,1024,256]{3,2,0,1:T(8,128)(2,1)S(1)} %get-tuple-element.4) | copy-start | bytes 3145732
  164.5 5.2 %copy-start.10 = (bf16[16,1,80,2048]{3,2,0,1:T(8,128)(2,1)S(1)}, bf16[16,1,80,2048]{3,2,0,1:T(8,128)(2,1)}, u32[]{:S(2)}) copy-start(bf16[16,1,80,2048]{3,2,0,1:T(8,128)(2,1)} %all-gather.5.cloned.1.call-done) | copy-start | bytes 15728644
  211.7 12.3 %copy-start.8 = (f32[256,4]{0,1:T(4,128)S(1)}, f32[256,4]{0,1:T(4,128)}, u32[]{:S(2)}) copy-start(f32[256,4]{0,1:T(4,128)} %param.9) | copy-start | bytes 12292
  216.6 25.5 %all-to-all-start.3 = ((bf16[1,16,80,256]{3,2,0,1:T(8,128)(2,1)}), bf16[1,16,80,256]{3,2,0,1:T(8,128)(2,1)S(1)}, u32[]{:S(2)}, u32[]{:S(2)}) async-start(bf16[1,16,80,256]{3,2,0,1:T(8,128)(2,1)} %fusion.21), calls=%async_computation.3 | async-start | bytes 1310720 | tf_op jit(solution)/shard_map/all_to_all | solution.py:118
Sparse Core Ops, SparseCore 0:
  44.7 40.7 all-gather.4
  172.5 39.1 all-gather.6
where the time goes:
time: 250 us
  blocking collectives  146 us (58%)
  waiting for transfers between devices  53 us (21%)
  matrix products  17.6 us (7%)
  between operations  14.4 us (6%)
  other arithmetic  8.79 us (4%)
  starting transfers between devices  7.45 us (3%)
    all_to_all x1, blocking collectives, from_everyone(): lax.all_to_all(jnp.broadcast_to(array[None], (devices, *array.shape)), ax...  77.2 us
    all_to_all x1, blocking collectives, sent_together(): lax.all_to_all(both, axis, split_axis=split_dim, concat_axis=concat_dim,...  41.3 us
    all_gather x1, waiting for transfers between devices, local(): lax.all_gather(hidden, 'tp', axis=3, tiled=True)  39.3 us
    all_to_all x1, blocking collectives, local(): lax.all_to_all(outgoing, 'fs', split_axis=0, concat_axis=1, tiled=True)  27.9 us
    all_to_all x1, waiting for transfers between devices, local(): lax.all_to_all(results, 'fs', split_axis=1, concat_axis=0, tiled=True)  13.6 us
    all_to_all x1, starting transfers between devices, local(): lax.all_to_all(results, 'fs', split_axis=1, concat_axis=0, tiled=True)  7.37 us
    dot_general x1, matrix products, local(): jnp.einsum('egnd,edf->egnf', portion, served_gate, preferred_element_type...  5.17 us
  transfers between devices with their start and end apart: 3, of which 2 were waited for; matrix products, arithmetic and copies ran while one was open for 2% of the time, Pallas kernels for 0%

commit v1 on v0

v1 whole, which is shorter than its diff:
```python
import jax
import jax.numpy as jnp
from jax import lax
from jax.experimental import pallas as pl
from jax.experimental.pallas import tpu as pltpu
from jax.sharding import PartitionSpec as P

MESH = pl.DeviceIdType.MESH
BF16, F32 = jnp.bfloat16, jnp.float32

EXPERTS = 16
TOP = 4
CAP = 80
ROWS = 256
SLOTS = EXPERTS * CAP
COLS = 256
TPS = 8
ZS, YS, XS = 8, 4, 4
OWN = 64
CHUNKS = 4
CHUNK = SLOTS // CHUNKS
HALF = CHUNK // 2

norm_eps = 1e-06
clamp_limit = 7.0
sigmoid_slope = 1.702


def rem(a, n):
    return lax.rem(a, n)


def kernel(
    tok_h, ids_h, sc_h, gain_h, gate_h, up_h, down_h,
    og, ou, od, om,
    tok_v, ids_v, sc_v, gain_v, gate_v, up_v, down_v,
    qt, wt, onehot, combine_t, normed, slots,
    wb1, wb2, rcv1, rcv2, ag1, ag2, acc, res, ret, mix_v,
    load_sem, out_sem, tok_send, tok_recv, w1_send, w2_send, w1_recv, w2_recv,
    ag1_send, ag2_send, ag1_recv, ag2_recv, ret_send, ret_recv,
):
    gr, fs, tp = lax.axis_index("gr"), lax.axis_index("fs"), lax.axis_index("tp")
    z, y = gr * 4 + fs // 4, rem(fs, 4)
    x, core = tp // 2, rem(tp, 2)
    me = z * YS + y

    def at(zz, yy):
        return (zz // 4, rem(zz, 4) * 4 + yy, tp)

    def along(xx, cc):
        return (gr, fs, xx * 2 + cc)

    x_right, x_left, x_far = rem(x + 1, XS), rem(x + 3, XS), rem(x + 2, XS)
    right, left, sib = along(x_right, core), along(x_left, core), along(x, 1 - core)

    def remote(src, dst, send, recv, device):
        return pltpu.make_async_remote_copy(
            src_ref=src, dst_ref=dst, send_sem=send, recv_sem=recv,
            device_id=device, device_id_type=MESH,
        )

    def landed(ref, sem):
        pltpu.make_async_copy(ref, ref, sem).wait()

    loads = [
        pltpu.make_async_copy(s, d, load_sem.at[i])
        for i, (s, d) in enumerate(
            ((ids_h, ids_v), (sc_h, sc_v), (tok_h, tok_v), (gain_h, gain_v),
             (gate_h, gate_v), (up_h, up_v), (down_h, down_v))
        )
    ]
    for c in loads:
        c.start()

    barrier = pltpu.get_barrier_semaphore()

    def greet(i, carry):
        zz, yy = rem(z + i // 4, ZS), rem(y + rem(i, 4), YS)
        pl.semaphore_signal(barrier, inc=1, device_id=at(zz, yy), device_id_type=MESH)
        return carry

    lax.fori_loop(1, ZS * YS, greet, 0)
    for d in (right, left, sib):
        pl.semaphore_signal(barrier, inc=1, device_id=d, device_id_type=MESH)

    loads[0].wait()
    loads[1].wait()
    ids = ids_v[...]
    exponent = jnp.exp(sc_v[...])
    total = jnp.sum(exponent, axis=0, keepdims=True)
    weights = (exponent / total).astype(BF16).astype(F32)
    expert_of = lax.broadcasted_iota(jnp.int32, (EXPERTS, ROWS), 0)
    member = jnp.zeros((EXPERTS, ROWS), F32)
    weight_of = jnp.zeros((EXPERTS, ROWS), F32)
    for k in range(TOP):
        same = ids[k : k + 1, :] == expert_of
        member = member + jnp.where(same, 1.0, 0.0)
        weight_of = weight_of + jnp.where(same, weights[k : k + 1, :], 0.0)
    earlier = jnp.where(
        lax.broadcasted_iota(jnp.int32, (ROWS, ROWS), 0)
        < lax.broadcasted_iota(jnp.int32, (ROWS, ROWS), 1),
        1.0, 0.0,
    ).astype(BF16)
    before = jnp.dot(member.astype(BF16), earlier, preferred_element_type=F32)
    qt[...] = jnp.where(member > 0.5, before, -1.0)
    wt[...] = weight_of

    slot_no = lax.broadcasted_iota(jnp.int32, (CAP, ROWS), 0).astype(F32)

    def tables(e, carry):
        hit = qt[pl.ds(e, 1), :] == slot_no
        rows = pl.ds(pl.multiple_of(e * CAP, 16), CAP)
        onehot[rows, :] = jnp.where(hit, 1.0, 0.0).astype(BF16)
        combine_t[rows, :] = jnp.where(hit, wt[pl.ds(e, 1), :], 0.0).astype(BF16)
        return carry

    lax.fori_loop(0, EXPERTS, tables, 0)

    loads[2].wait()

    def norm(i, carry):
        rows = pl.ds(pl.multiple_of(i * 32, 32), 32)
        full = tok_v[rows, :].astype(F32)
        scale = lax.rsqrt(jnp.mean(full * full, axis=1, keepdims=True) + norm_eps)
        mine = tok_v[rows, pl.ds(pl.multiple_of(tp * COLS, COLS), COLS)].astype(F32)
        normed[rows, :] = (mine * scale).astype(BF16)
        return carry

    lax.fori_loop(0, ROWS // 32, norm, 0)

    def fill(i, carry):
        rows = pl.ds(pl.multiple_of(i * CHUNK, CHUNK), CHUNK)
        slots[rows, :] = jnp.dot(
            onehot[rows, :], normed[...], preferred_element_type=F32
        ).astype(BF16)
        return carry

    lax.fori_loop(0, CHUNKS, fill, 0)

    loads[3].wait()
    square = (OWN, OWN)
    gain = jnp.sum(
        jnp.where(
            lax.broadcasted_iota(jnp.int32, square, 0) == lax.broadcasted_iota(jnp.int32, square, 1),
            jnp.broadcast_to(gain_v[...], square), 0.0,
        ),
        axis=1, keepdims=True,
    )
    for i in (4, 5, 6):
        loads[i].wait()

    def fold(e, carry):
        wb1[e, :, 0:COLS] = (gain * gate_v[e]).astype(BF16)
        wb1[e, :, COLS : 2 * COLS] = (gain * up_v[e]).astype(BF16)
        wb2[e] = down_v[e].astype(BF16)
        return carry

    lax.fori_loop(0, EXPERTS, fold, 0)
    own_rows = pl.ds(pl.multiple_of(me * OWN, OWN), OWN)
    rcv1[own_rows, :] = wb1[fs]
    rcv2[own_rows, :] = wb2[fs]

    def slot_rows(e):
        return pl.ds(pl.multiple_of(e * CAP, 16), CAP)

    self_slot = 3 * 4 + y
    ag1[tp, slot_rows(self_slot), :] = slots[slot_rows(fs), :]

    pl.semaphore_wait(barrier, ZS * YS - 1 + 3)

    def send_slots(zt, yt, group):
        e = rem(zt, 4) * 4 + yt
        remote(
            slots.at[slot_rows(e)], ag1.at[tp, slot_rows(group * 4 + y)],
            tok_send, tok_recv, at(zt, yt),
        ).start()

    def two_away(yt, carry):
        step = jnp.where(rem(y + yt, 2) == 0, 2, 6)
        send_slots(rem(z + step, ZS), yt, 0)
        return carry

    lax.fori_loop(0, YS, two_away, 0)

    def one_away(yt, carry):
        send_slots(rem(z + 1, ZS), yt, 1)
        send_slots(rem(z + 7, ZS), yt, 2)
        return carry

    lax.fori_loop(0, YS, one_away, 0)

    def same_plane(i, carry):
        send_slots(z, rem(y + i, YS), 3)
        return carry

    lax.fori_loop(1, YS, same_plane, 0)

    def plane(k):
        away = (k + 1) // 2
        return rem(z + jnp.where(rem(k, 2) == 1, away, ZS - away), ZS)

    def send_weights(source, landing, send, recv):
        def one(i, carry):
            zt, yt = plane(i // 4), rem(y + rem(i, 4), YS)
            remote(
                source.at[rem(zt, 4) * 4 + yt], landing.at[own_rows],
                send, recv.at[z], at(zt, yt),
            ).start()
            return carry

        lax.fori_loop(1, ZS * YS, one, 0)

    send_weights(wb1, rcv1, w1_send, w1_recv)
    send_weights(wb2, rcv2, w2_send, w2_recv)

    def chunk_rows(q):
        return pl.ds(q * CHUNK, CHUNK)

    def gather(buf, send, recv):
        def own(q):
            piece = buf.at[tp, chunk_rows(q)]
            remote(piece, piece, send, recv.at[0, q], right).start()
            remote(piece, piece, send, recv.at[1, q], left).start()
            remote(piece, piece, send, recv.at[4, q], sib).start()

        def forward(q):
            from_left = buf.at[x_left * 2 + core, chunk_rows(q)]
            landed(from_left, recv.at[0, q])
            first = buf.at[x_left * 2 + core, pl.ds(q * CHUNK, HALF)]
            remote(first, first, send, recv.at[2, q], right).start()
            remote(from_left, from_left, send, recv.at[5, q], sib).start()
            from_right = buf.at[x_right * 2 + core, chunk_rows(q)]
            landed(from_right, recv.at[1, q])
            second = buf.at[x_right * 2 + core, pl.ds(q * CHUNK + HALF, HALF)]
            remote(second, second, send, recv.at[3, q], left).start()
            remote(from_right, from_right, send, recv.at[6, q], sib).start()

        def far(q):
            landed(buf.at[x_far * 2 + core, pl.ds(q * CHUNK, HALF)], recv.at[2, q])
            landed(buf.at[x_far * 2 + core, pl.ds(q * CHUNK + HALF, HALF)], recv.at[3, q])
            piece = buf.at[x_far * 2 + core, chunk_rows(q)]
            remote(piece, piece, send, recv.at[7, q], sib).start()

        def others(q):
            for i, xx in ((4, x), (5, x_left), (6, x_right), (7, x_far)):
                landed(buf.at[xx * 2 + 1 - core, chunk_rows(q)], recv.at[i, q])

        return own, forward, far, others

    own, forward, far, others = gather(ag1, ag1_send, ag1_recv)
    landed(ag1.at[0, pl.ds(0, SLOTS - CAP)], tok_recv)
    own(0)
    own(1)
    for q in range(CHUNKS):
        forward(q)
        if q + 2 < CHUNKS:
            own(q + 2)
    for q in range(CHUNKS):
        far(q)
    for q in range(CHUNKS):
        others(q)

    def dot_rows(j, rows):
        return jnp.dot(
            ag1[j, rows, :], rcv1[pl.ds(pl.multiple_of(j * COLS, COLS), COLS), :],
            preferred_element_type=F32,
        )

    def spread(r):
        return pl.ds(pl.multiple_of(r * CHUNK, CHUNK), CHUNK)

    landed(rcv1.at[pl.ds(0, 3 * OWN)], w1_recv.at[z])

    def first_plane(r, carry):
        acc[spread(r), :] = dot_rows(z, spread(r))
        return carry

    lax.fori_loop(0, CHUNKS, first_plane, 0)

    def next_plane(k, carry):
        j = plane(k)
        landed(rcv1.at[pl.ds(0, 4 * OWN)], w1_recv.at[j])

        def more(r, inner):
            acc[spread(r), :] += dot_rows(j, spread(r))
            return inner

        return lax.fori_loop(0, CHUNKS, more, carry)

    lax.fori_loop(1, ZS - 1, next_plane, 0)
    last = plane(ZS - 1)
    landed(rcv1.at[pl.ds(0, 4 * OWN)], w1_recv.at[last])

    own, forward, far, others = gather(ag2, ag2_send, ag2_recv)

    def produce(q):
        rows = chunk_rows(q)
        pre = acc[rows, :] + dot_rows(last, rows)
        g = jnp.minimum(pre[:, :COLS], clamp_limit)
        v = jnp.clip(pre[:, COLS:], -clamp_limit, clamp_limit)
        ag2[tp, rows, :] = (g * jax.nn.sigmoid(sigmoid_slope * g) * (v + 1.0)).astype(BF16)

    produce(0)
    own(0)
    produce(1)
    own(1)
    produce(2)
    produce(3)
    outs = [
        pltpu.make_async_copy(rcv1.at[:, pl.ds(0, COLS)], og.at[0], out_sem.at[0]),
        pltpu.make_async_copy(rcv1.at[:, pl.ds(COLS, COLS)], ou.at[0], out_sem.at[1]),
        pltpu.make_async_copy(rcv2, od.at[0], out_sem.at[2]),
    ]
    outs[0].start()
    outs[1].start()
    for q in range(CHUNKS):
        forward(q)
        if q + 2 < CHUNKS:
            own(q + 2)
    for q in range(CHUNKS):
        far(q)

    landed(rcv2.at[pl.ds(0, 3 * OWN)], w2_recv.at[z])

    def down_landed(k, carry):
        landed(rcv2.at[pl.ds(0, 4 * OWN)], w2_recv.at[plane(k)])
        return carry

    lax.fori_loop(1, ZS, down_landed, 0)
    outs[2].start()

    def finish(q):
        others(q)
        rows = chunk_rows(q)
        summed = jnp.zeros((CHUNK, COLS), F32)
        for j in range(TPS):
            summed = summed + jnp.dot(
                ag2[j, rows, :], rcv2[j * COLS : (j + 1) * COLS, :], preferred_element_type=F32
            )
        res[rows, :] = summed.astype(BF16)

    def send_back(group, ys, zs):
        remote(
            res.at[slot_rows(group * 4 + ys)], ret.at[slot_rows(fs)],
            ret_send, ret_recv, at(zs, ys),
        ).start()

    def back_two(ys, carry):
        step = jnp.where(rem(y + ys, 2) == 0, 6, 2)
        send_back(0, ys, rem(z + step, ZS))
        return carry

    finish(0)
    lax.fori_loop(0, YS, back_two, 0)

    def back_left(ys, carry):
        send_back(1, ys, rem(z + 7, ZS))
        return carry

    finish(1)
    lax.fori_loop(0, YS, back_left, 0)

    def back_right(ys, carry):
        send_back(2, ys, rem(z + 1, ZS))
        return carry

    finish(2)
    lax.fori_loop(0, YS, back_right, 0)

    def back_here(i, carry):
        send_back(3, rem(y + i, YS), z)
        return carry

    finish(3)
    lax.fori_loop(1, YS, back_here, 0)
    ret[slot_rows(fs), :] = res[slot_rows(self_slot), :]

    landed(ret.at[pl.ds(0, SLOTS - CAP)], ret_recv)
    mix_v[...] = lax.dot_general(
        combine_t[...], ret[...], (((0,), (0,)), ((), ())), preferred_element_type=F32
    ).astype(BF16)
    mix_out = pltpu.make_async_copy(mix_v, om, out_sem.at[3])
    mix_out.start()

    landed(slots.at[pl.ds(0, SLOTS - CAP)], tok_send)
    landed(ret.at[pl.ds(0, SLOTS - CAP)], ret_send)
    landed(rcv1.at[pl.ds(0, 31 * OWN)], w1_send)
    landed(rcv2.at[pl.ds(0, 31 * OWN)], w2_send)
    landed(ag1.at[pl.ds(0, 7)], ag1_send)
    landed(ag2.at[pl.ds(0, 7)], ag2_send)
    for c in outs:
        c.wait()
    mix_out.wait()


def local(tokens, route_ids, route_scores, norm_gain, gate_weight, up_weight, down_weight):
    anywhere = pl.BlockSpec(memory_space=pl.ANY)
    dma = pltpu.SemaphoreType.DMA
    served = jax.ShapeDtypeStruct((1, 2048, COLS), BF16)
    return pl.pallas_call(
        kernel,
        name="hand_over",
        out_shape=(served, served, served, jax.ShapeDtypeStruct((ROWS, COLS), BF16)),
        in_specs=[anywhere] * 7,
        out_specs=[anywhere] * 4,
        scratch_shapes=[
            pltpu.VMEM((ROWS, 2048), BF16),
            pltpu.VMEM((TOP, ROWS), jnp.int32),
            pltpu.VMEM((TOP, ROWS), F32),
            pltpu.VMEM((1, OWN), F32),
            pltpu.VMEM((EXPERTS, OWN, COLS), F32),
            pltpu.VMEM((EXPERTS, OWN, COLS), F32),
            pltpu.VMEM((EXPERTS, OWN, COLS), F32),
            pltpu.VMEM((EXPERTS, ROWS), F32),
            pltpu.VMEM((EXPERTS, ROWS), F32),
            pltpu.VMEM((SLOTS, ROWS), BF16),
            pltpu.VMEM((SLOTS, ROWS), BF16),
            pltpu.VMEM((ROWS, COLS), BF16),
            pltpu.VMEM((SLOTS, COLS), BF16),
            pltpu.VMEM((EXPERTS, OWN, 2 * COLS), BF16),
            pltpu.VMEM((EXPERTS, OWN, COLS), BF16),
            pltpu.VMEM((2048, 2 * COLS), BF16),
            pltpu.VMEM((2048, COLS), BF16),
            pltpu.VMEM((TPS, SLOTS, COLS), BF16),
            pltpu.VMEM((TPS, SLOTS, COLS), BF16),
            pltpu.VMEM((SLOTS, 2 * COLS), F32),
            pltpu.VMEM((SLOTS, COLS), BF16),
            pltpu.VMEM((SLOTS, COLS), BF16),
            pltpu.VMEM((ROWS, COLS), BF16),
            dma((7,)), dma((4,)), dma(()), dma(()), dma(()), dma(()), dma((ZS,)), dma((ZS,)),
            dma(()), dma(()), dma((8, CHUNKS)), dma((8, CHUNKS)), dma(()), dma(()),
        ],
        compiler_params=pltpu.CompilerParams(
            collective_id=0, has_side_effects=True, vmem_limit_bytes=56 * 1024 * 1024
        ),
    )(
        tokens, route_ids.T, route_scores.T, norm_gain.reshape(1, OWN),
        gate_weight, up_weight, down_weight,
    )


def solution(mesh):
    in_specs = (
        P(("gr", "fs"), None),
        P(("gr", "fs"), None),
        P(("gr", "fs"), None),
        P(("gr", "fs")),
        P(None, ("gr", "fs"), "tp"),
        P(None, ("gr", "fs"), "tp"),
        P(None, ("gr", "fs"), "tp"),
    )
    out_specs = (
        P("fs", None, "tp"),
        P("fs", None, "tp"),
        P("fs", None, "tp"),
        P(("gr", "fs"), "tp"),
    )
    return jax.shard_map(local, mesh=mesh, in_specs=in_specs, out_specs=out_specs, check_vma=False)
```

time: 250 us -> 111 us (0.44)
  blocking collectives: 146 us -> 0 us
  Pallas kernels: 0 us -> 103 us
  waiting for transfers between devices: 53 us -> 0 us
  matrix products: 17.6 us -> 0 us
  between operations: 14.4 us -> 0.65 us
  other arithmetic: 8.79 us -> 0 us
  starting transfers between devices: 7.45 us -> 0 us
  local copies, waits for them, and re-layouts: 2.3 us -> 5.63 us
    all_to_all x3 -> x0, blocking collectives: 146 us -> none  [the longest x1 77.2 us: from_everyone(): lax.all_to_all(jnp.broadcast_to(array[None], (devices, *array.shape)), ax...]
    pallas_call x0 -> x1, Pallas kernels: none -> 103 us  [local(): pl.pallas_call(kernel, name='hand_over', out_shape=(served, served, serve...]
    all_gather x2 -> x0, waiting for transfers between devices: 39.3 us -> none  [the longest x1 39.3 us: local(): lax.all_gather(hidden, 'tp', axis=3, tiled=True)]
    dot_general x6 -> x0, matrix products: 17.6 us -> none  [the longest x1 5.17 us: local(): jnp.einsum('egnd,edf->egnf', portion, served_gate, preferred_element_type...]
    all_to_all x1 -> x0, waiting for transfers between devices: 13.6 us -> none  [local(): lax.all_to_all(results, 'fs', split_axis=1, concat_axis=0, tiled=True)]
    all_to_all x1 -> x0, starting transfers between devices: 7.37 us -> none  [local(): lax.all_to_all(results, 'fs', split_axis=1, concat_axis=0, tiled=True)]
    unnamed x23 -> x10, local copies, waits for them, and re-layouts: 0.88 us -> 5.63 us
    another operation x3 -> x0, other arithmetic: 4.64 us -> none
  transfers between devices with their start and end apart: 3 -> 0, of which waited for: 2 -> 0; matrix products, arithmetic and copies ran while one was open for 2% -> 0% of each run, Pallas kernels for 0% -> 0%
where the time goes in v1:
time: 111 us; the launch traced here: 109 us
  Pallas kernels  103 us (93%)
  local copies, waits for them, and re-layouts  5.63 us (5%)
    pallas_call x1, Pallas kernels, local(): pl.pallas_call(kernel, name='hand_over', out_shape=(served, served, serve...  103 us
    unnamed x10, local copies, waits for them, and re-layouts  5.63 us

profile of v1, /device:TPU:4, one launch (start us, length us, event | category | flops | bytes accessed | tf_op | source)
XLA Modules:
  0.0 108.9 jit_solution(13372788061154298600)
XLA Ops:
  0.6 102.6 %hand_over.1 = (bf16[1,2048,256]{2,1,0:T(8,128)(2,1)}, bf16[1,2048,256]{2,1,0:T(8,128)(2,1)}, bf16[1,2048,256]{2,1,0:T(8,128)(2,1)}, bf16[256,256]{1,0:T(8,128)(2,1)}) custom-call(bf16[256,2048]{1,0:T(8,128)(2,1)} %tok_h.1, s32[4,256]{1,0:T(4,128)} %bitcast.3, f32[4,256]{1,0:T(4,128)} %bitcast.4, f32[1,64]{1,0:T(1,128)} %bitcast.5, f32[16,64,256]{2,1,0:T(8,128)} %gate_h.1, ...), custom_call_target="tpu_custom_call" | custom-call | tf_op jit(solution)/shard_map/hand_over/pallas_call | solution.py:400
  103.3 0.0 copy-start.1
  103.3 2.4 %copy.15 = bf16[1,2048,256]{2,1,0:T(8,128)(2,1)} copy(bf16[1,2048,256]{2,1,0:T(8,128)(2,1)} %get-tuple-element.8) | data formatting | bytes 2097152
  105.6 0.0 copy-done.1
  105.6 0.0 copy-start
  105.6 1.0 copy.16
  106.6 0.6 copy-done
  107.2 0.0 copy-start.2
  107.2 1.0 copy.17
  108.2 0.1 copy-done.2
  108.3 0.7 copy.18
Async XLA Ops:
  103.3 2.4 %copy-start.1 = (bf16[1,2048,256]{2,1,0:T(8,128)(2,1)S(1)}, bf16[1,2048,256]{2,1,0:T(8,128)(2,1)}, u32[]{:S(2)}) copy-start(bf16[1,2048,256]{2,1,0:T(8,128)(2,1)} %get-tuple-element.9) | copy-start | bytes 3145732
  105.6 1.6 %copy-start = (bf16[1,2048,256]{2,1,0:T(8,128)(2,1)S(1)}, bf16[1,2048,256]{2,1,0:T(8,128)(2,1)}, u32[]{:S(2)}) copy-start(bf16[1,2048,256]{2,1,0:T(8,128)(2,1)} %get-tuple-element.10) | copy-start | bytes 3145732
  107.2 1.0 copy-start.2

commit v2 on v1

v2 whole, which is shorter than its diff:
```python
import jax
import jax.numpy as jnp
from jax import lax
from jax.experimental import pallas as pl
from jax.experimental.pallas import tpu as pltpu
from jax.sharding import PartitionSpec as P

MESH = pl.DeviceIdType.MESH
BF16, F32 = jnp.bfloat16, jnp.float32

EXPERTS = 16
TOP = 4
CAP = 80
ROWS = 256
SLOTS = EXPERTS * CAP
COLS = 256
SIDE = COLS // 2
TPS = 8
ZS, YS, XS = 8, 4, 4
OWN = 64
CHUNKS = 4
CHUNK = SLOTS // CHUNKS
HALF = CHUNK // 2
EARLY = 5

norm_eps = 1e-06
clamp_limit = 7.0
sigmoid_slope = 1.702


def rem(a, n):
    return lax.rem(a, n)


def kernel(
    tok_h, ids_h, sc_h, gain_h, gate_h, up_h, down_h,
    rcv1a, rcv1b, rcv2, ret, combine_t,
    tok_v, ids_v, sc_v, gain_v, gate_v, up_v, down_v,
    qt, wt, onehot, normed, slots,
    wb1a, wb1b, wb2, ag1, ag2, acc, res,
    load_sem, tok_send, tok_recv, w_send, w1a_recv, w1b_recv, w2_recv,
    ag_send, ag1_recv, ag2a_recv, ag2b_recv, ret_send, ret_recv,
):
    gr, fs, tp = lax.axis_index("gr"), lax.axis_index("fs"), lax.axis_index("tp")
    z, y = gr * 4 + fs // 4, rem(fs, 4)
    x, core = tp // 2, rem(tp, 2)
    me = z * YS + y

    def at(zz, yy):
        return (zz // 4, rem(zz, 4) * 4 + yy, tp)

    def along(xx, cc):
        return (gr, fs, xx * 2 + cc)

    x_right, x_left, x_far = rem(x + 1, XS), rem(x + 3, XS), rem(x + 2, XS)
    right, left, sib = along(x_right, core), along(x_left, core), along(x, 1 - core)

    def remote(src, dst, send, recv, device):
        return pltpu.make_async_remote_copy(
            src_ref=src, dst_ref=dst, send_sem=send, recv_sem=recv,
            device_id=device, device_id_type=MESH,
        )

    def landed(ref, sem):
        pltpu.make_async_copy(ref, ref, sem).wait()

    loads = [
        pltpu.make_async_copy(s, d, load_sem.at[i])
        for i, (s, d) in enumerate(
            ((ids_h, ids_v), (sc_h, sc_v), (tok_h, tok_v), (gain_h, gain_v),
             (gate_h, gate_v), (up_h, up_v), (down_h, down_v))
        )
    ]
    for c in loads:
        c.start()

    barrier = pltpu.get_barrier_semaphore()

    def greet(i, carry):
        zz, yy = rem(z + i // 4, ZS), rem(y + rem(i, 4), YS)
        pl.semaphore_signal(barrier, inc=1, device_id=at(zz, yy), device_id_type=MESH)
        return carry

    lax.fori_loop(1, ZS * YS, greet, 0)
    for d in (right, left, sib):
        pl.semaphore_signal(barrier, inc=1, device_id=d, device_id_type=MESH)

    loads[0].wait()
    loads[1].wait()
    ids = ids_v[...]
    exponent = jnp.exp(sc_v[...])
    total = jnp.sum(exponent, axis=0, keepdims=True)
    weights = (exponent / total).astype(BF16).astype(F32)
    expert_of = lax.broadcasted_iota(jnp.int32, (EXPERTS, ROWS), 0)
    member = jnp.zeros((EXPERTS, ROWS), F32)
    weight_of = jnp.zeros((EXPERTS, ROWS), F32)
    for k in range(TOP):
        same = ids[k : k + 1, :] == expert_of
        member = member + jnp.where(same, 1.0, 0.0)
        weight_of = weight_of + jnp.where(same, weights[k : k + 1, :], 0.0)
    earlier = jnp.where(
        lax.broadcasted_iota(jnp.int32, (ROWS, ROWS), 0)
        < lax.broadcasted_iota(jnp.int32, (ROWS, ROWS), 1),
        1.0, 0.0,
    ).astype(BF16)
    before = jnp.dot(member.astype(BF16), earlier, preferred_element_type=F32)
    qt[...] = jnp.where(member > 0.5, before, -1.0)
    wt[...] = weight_of

    slot_no = lax.broadcasted_iota(jnp.int32, (CAP, ROWS), 0).astype(F32)

    def tables(e, carry):
        hit = qt[pl.ds(e, 1), :] == slot_no
        rows = pl.ds(pl.multiple_of(e * CAP, 16), CAP)
        onehot[rows, :] = jnp.where(hit, 1.0, 0.0).astype(BF16)
        combine_t[rows, :] = jnp.where(hit, wt[pl.ds(e, 1), :], 0.0).astype(BF16)
        return carry

    lax.fori_loop(0, EXPERTS, tables, 0)

    loads[2].wait()

    def norm(i, carry):
        rows = pl.ds(pl.multiple_of(i * 32, 32), 32)
        full = tok_v[rows, :].astype(F32)
        scale = lax.rsqrt(jnp.mean(full * full, axis=1, keepdims=True) + norm_eps)
        mine = tok_v[rows, pl.ds(pl.multiple_of(tp * COLS, COLS), COLS)].astype(F32)
        normed[rows, :] = (mine * scale).astype(BF16)
        return carry

    lax.fori_loop(0, ROWS // 32, norm, 0)

    def fill(i, carry):
        rows = pl.ds(pl.multiple_of(i * CHUNK, CHUNK), CHUNK)
        slots[rows, :] = jnp.dot(
            onehot[rows, :], normed[...], preferred_element_type=F32
        ).astype(BF16)
        return carry

    lax.fori_loop(0, CHUNKS, fill, 0)

    loads[3].wait()
    square = (OWN, OWN)
    gain = jnp.sum(
        jnp.where(
            lax.broadcasted_iota(jnp.int32, square, 0) == lax.broadcasted_iota(jnp.int32, square, 1),
            jnp.broadcast_to(gain_v[...], square), 0.0,
        ),
        axis=1, keepdims=True,
    )
    for i in (4, 5, 6):
        loads[i].wait()

    def fold(e, carry):
        gate, up = (gain * gate_v[e]).astype(BF16), (gain * up_v[e]).astype(BF16)
        wb1a[e, :, 0:SIDE] = gate[:, :SIDE]
        wb1a[e, :, SIDE:COLS] = up[:, :SIDE]
        wb1b[e, :, 0:SIDE] = gate[:, SIDE:]
        wb1b[e, :, SIDE:COLS] = up[:, SIDE:]
        wb2[e] = down_v[e].astype(BF16)
        return carry

    lax.fori_loop(0, EXPERTS, fold, 0)
    own_rows = pl.ds(pl.multiple_of(me * OWN, OWN), OWN)
    rcv1a[own_rows, :] = wb1a[fs]
    rcv1b[own_rows, :] = wb1b[fs]
    rcv2[own_rows, :] = wb2[fs]

    def slot_rows(e):
        return pl.ds(pl.multiple_of(e * CAP, 16), CAP)

    self_slot = 3 * 4 + y
    ag1[tp, slot_rows(self_slot), :] = slots[slot_rows(fs), :]

    pl.semaphore_wait(barrier, ZS * YS - 1 + 3)

    def send_slots(zt, yt, group):
        e = rem(zt, 4) * 4 + yt
        remote(
            slots.at[slot_rows(e)], ag1.at[tp, slot_rows(group * 4 + y)],
            tok_send, tok_recv.at[group], at(zt, yt),
        ).start()

    def same_plane(i, carry):
        send_slots(z, rem(y + i, YS), 3)
        return carry

    lax.fori_loop(1, YS, same_plane, 0)

    def one_away(yt, carry):
        send_slots(rem(z + 1, ZS), yt, 1)
        send_slots(rem(z + 7, ZS), yt, 2)
        return carry

    lax.fori_loop(0, YS, one_away, 0)

    def two_away(yt, carry):
        step = jnp.where(rem(y + yt, 2) == 0, 2, 6)
        send_slots(rem(z + step, ZS), yt, 0)
        return carry

    lax.fori_loop(0, YS, two_away, 0)

    def plane(k):
        away = (k + 1) // 2
        return rem(z + jnp.where(rem(k, 2) == 1, away, ZS - away), ZS)

    def send_weights(source, landing, send, recv):
        def one(i, carry):
            zt, yt = plane(i // 4), rem(y + rem(i, 4), YS)
            remote(
                source.at[rem(zt, 4) * 4 + yt], landing.at[own_rows],
                send, recv.at[z], at(zt, yt),
            ).start()
            return carry

        lax.fori_loop(1, ZS * YS, one, 0)

    send_weights(wb1a, rcv1a, w_send.at[0], w1a_recv)
    send_weights(wb1b, rcv1b, w_send.at[1], w1b_recv)
    send_weights(wb2, rcv2, w_send.at[2], w2_recv)

    def gather(buf, columns, send, recv):
        def piece(xx, cc, start, size):
            return buf.at[xx * 2 + cc, pl.ds(start, size), columns]

        def own(q):
            mine = piece(x, core, q * CHUNK, CHUNK)
            remote(mine, mine, send, recv.at[0, q], right).start()
            remote(mine, mine, send, recv.at[1, q], left).start()
            remote(mine, mine, send, recv.at[4, q], sib).start()

        def forward(q):
            whole = piece(x_left, core, q * CHUNK, CHUNK)
            landed(whole, recv.at[0, q])
            first = piece(x_left, core, q * CHUNK, HALF)
            remote(first, first, send, recv.at[2, q], right).start()
            remote(whole, whole, send, recv.at[5, q], sib).start()
            whole = piece(x_right, core, q * CHUNK, CHUNK)
            landed(whole, recv.at[1, q])
            second = piece(x_right, core, q * CHUNK + HALF, HALF)
            remote(second, second, send, recv.at[3, q], left).start()
            remote(whole, whole, send, recv.at[6, q], sib).start()

        def far(q):
            landed(piece(x_far, core, q * CHUNK, HALF), recv.at[2, q])
            landed(piece(x_far, core, q * CHUNK + HALF, HALF), recv.at[3, q])
            whole = piece(x_far, core, q * CHUNK, CHUNK)
            remote(whole, whole, send, recv.at[7, q], sib).start()

        def others(q):
            for i, xx in ((4, x), (5, x_left), (6, x_right), (7, x_far)):
                landed(piece(xx, 1 - core, q * CHUNK, CHUNK), recv.at[i, q])

        def run(order, prepare):
            for i in range(CHUNKS + 3):
                if i < CHUNKS:
                    prepare(order[i])
                    own(order[i])
                if 0 <= i - 2 < CHUNKS:
                    forward(order[i - 2])
                if 0 <= i - 4:
                    far(order[i - 4])
            far(order[CHUNKS - 1])
            for q in range(CHUNKS):
                others(q)

        return run

    def group_landed(q):
        landed(ag1.at[0, pl.ds(0, (3 if q == 3 else 4) * CAP)], tok_recv.at[q])

    gather(ag1, pl.ds(0, COLS), ag_send.at[0], ag1_recv)((3, 1, 2, 0), group_landed)

    def planes_landed(landing, recv, first, end):
        if first == 0:
            landed(landing.at[pl.ds(0, 3 * OWN)], recv.at[z])

        def one(k, carry):
            landed(landing.at[pl.ds(0, 4 * OWN)], recv.at[plane(k)])
            return carry

        lax.fori_loop(max(first, 1), end, one, 0)

    def product(left_of, right_of, rows, ks):
        total = None
        for k in ks:
            j = plane(k) if isinstance(ks, tuple) else k
            start = pl.multiple_of(j * COLS, COLS) if isinstance(ks, tuple) else k * COLS
            part = jnp.dot(
                left_of[j, rows, :], right_of[pl.ds(start, COLS), :], preferred_element_type=F32
            )
            total = part if total is None else total + part
        return total

    def half(landing, side, send, recv, hidden_recv):
        columns = pl.ds(side * SIDE, SIDE)

        def hidden(q):
            rows = pl.ds(q * CHUNK, CHUNK)
            pre = product(ag1, landing, rows, range(ZS))
            g = jnp.minimum(pre[:, :SIDE], clamp_limit)
            v = jnp.clip(pre[:, SIDE:], -clamp_limit, clamp_limit)
            ag2[tp, rows, columns] = (g * jax.nn.sigmoid(sigmoid_slope * g) * (v + 1.0)).astype(BF16)

        planes_landed(landing, recv, 0, ZS)
        gather(ag2, columns, send, hidden_recv)(tuple(range(CHUNKS)), hidden)

    half(rcv1a, 0, ag_send.at[1], w1a_recv, ag2a_recv)
    half(rcv1b, 1, ag_send.at[2], w1b_recv, ag2b_recv)

    def send_back(group, ys, zs):
        remote(
            res.at[slot_rows(group * 4 + ys)], ret.at[slot_rows(fs)],
            ret_send, ret_recv, at(zs, ys),
        ).start()

    def back(group):
        def one(i, carry):
            if group == 0:
                step = jnp.where(rem(y + i, 2) == 0, 6, 2)
                send_back(0, i, rem(z + step, ZS))
            elif group < 3:
                send_back(group, i, rem(z + (7 if group == 1 else 1), ZS))
            else:
                send_back(3, rem(y + i, YS), z)
            return carry

        lax.fori_loop(1 if group == 3 else 0, YS, one, 0)

    planes_landed(rcv2, w2_recv, 0, EARLY)

    def begin(r, carry):
        rows = pl.ds(pl.multiple_of(r * CHUNK, CHUNK), CHUNK)
        acc[rows, :] = product(ag2, rcv2, rows, tuple(range(EARLY)))
        return carry

    lax.fori_loop(0, CHUNKS, begin, 0)
    planes_landed(rcv2, w2_recv, EARLY, ZS)
    for r in range(CHUNKS):
        rows = pl.ds(r * CHUNK, CHUNK)
        res[rows, :] = (acc[rows, :] + product(ag2, rcv2, rows, tuple(range(EARLY, ZS)))).astype(BF16)
        back(r)
    ret[slot_rows(fs), :] = res[slot_rows(self_slot), :]

    landed(ret.at[pl.ds(0, SLOTS - CAP)], ret_recv)
    landed(slots.at[pl.ds(0, SLOTS - CAP)], tok_send)
    landed(ret.at[pl.ds(0, SLOTS - CAP)], ret_send)
    for i, landing in enumerate((rcv1a, rcv1b, rcv2)):
        landed(landing.at[pl.ds(0, 31 * OWN)], w_send.at[i])
    landed(ag1.at[pl.ds(0, 7)], ag_send.at[0])
    landed(ag2.at[pl.ds(0, 7), :, pl.ds(0, SIDE)], ag_send.at[1])
    landed(ag2.at[pl.ds(0, 7), :, pl.ds(0, SIDE)], ag_send.at[2])


def write_out(rcv1a, rcv1b, rcv2, ret, combine_t, og, ou, od, om, mix_v, sem):
    low, high = pl.ds(0, SIDE), pl.ds(SIDE, SIDE)
    copies = [
        pltpu.make_async_copy(s, d, sem.at[i])
        for i, (s, d) in enumerate((
            (rcv1a.at[:, low], og.at[0, :, low]), (rcv1b.at[:, low], og.at[0, :, high]),
            (rcv1a.at[:, high], ou.at[0, :, low]), (rcv1b.at[:, high], ou.at[0, :, high]),
            (rcv2, od.at[0]),
        ))
    ]
    for c in copies:
        c.start()
    mix_v[...] = lax.dot_general(
        combine_t[...], ret[...], (((0,), (0,)), ((), ())), preferred_element_type=F32
    ).astype(BF16)
    mix_out = pltpu.make_async_copy(mix_v, om, sem.at[5])
    mix_out.start()
    for c in copies:
        c.wait()
    mix_out.wait()


def local(tokens, route_ids, route_scores, norm_gain, gate_weight, up_weight, down_weight):
    hbm, vmem = pl.BlockSpec(memory_space=pltpu.HBM), pl.BlockSpec(memory_space=pltpu.VMEM)
    dma = pltpu.SemaphoreType.DMA
    rows = jax.ShapeDtypeStruct((2048, COLS), BF16)
    slots = jax.ShapeDtypeStruct((SLOTS, COLS), BF16)
    landed = pl.pallas_call(
        kernel,
        name="hand_over",
        out_shape=(rows, rows, rows, slots, slots),
        in_specs=[hbm] * 7,
        out_specs=[vmem] * 5,
        scratch_shapes=[
            pltpu.VMEM((ROWS, 2048), BF16),
            pltpu.VMEM((TOP, ROWS), jnp.int32),
            pltpu.VMEM((TOP, ROWS), F32),
            pltpu.VMEM((1, OWN), F32),
            pltpu.VMEM((EXPERTS, OWN, COLS), F32),
            pltpu.VMEM((EXPERTS, OWN, COLS), F32),
            pltpu.VMEM((EXPERTS, OWN, COLS), F32),
            pltpu.VMEM((EXPERTS, ROWS), F32),
            pltpu.VMEM((EXPERTS, ROWS), F32),
            pltpu.VMEM((SLOTS, ROWS), BF16),
            pltpu.VMEM((ROWS, COLS), BF16),
            pltpu.VMEM((SLOTS, COLS), BF16),
            pltpu.VMEM((EXPERTS, OWN, COLS), BF16),
            pltpu.VMEM((EXPERTS, OWN, COLS), BF16),
            pltpu.VMEM((EXPERTS, OWN, COLS), BF16),
            pltpu.VMEM((TPS, SLOTS, COLS), BF16),
            pltpu.VMEM((TPS, SLOTS, COLS), BF16),
            pltpu.VMEM((SLOTS, COLS), F32),
            pltpu.VMEM((SLOTS, COLS), BF16),
            dma((7,)), dma(()), dma((4,)), dma((3,)), dma((ZS,)), dma((ZS,)), dma((ZS,)),
            dma((3,)), dma((8, CHUNKS)), dma((8, CHUNKS)), dma((8, CHUNKS)), dma(()), dma(()),
        ],
        compiler_params=pltpu.CompilerParams(
            collective_id=0, has_side_effects=True, vmem_limit_bytes=52 * 1000 * 1000
        ),
    )(
        *(
            pltpu.with_memory_space_constraint(a, pltpu.HBM)
            for a in (tokens, route_ids.T, route_scores.T, norm_gain.reshape(1, OWN),
                      gate_weight, up_weight, down_weight)
        )
    )
    served = jax.ShapeDtypeStruct((1, 2048, COLS), BF16)
    return pl.pallas_call(
        write_out,
        name="write_out",
        out_shape=(served, served, served, jax.ShapeDtypeStruct((ROWS, COLS), BF16)),
        in_specs=[vmem] * 5,
        out_specs=[hbm] * 4,
        scratch_shapes=[pltpu.VMEM((ROWS, COLS), BF16), dma((6,))],
        compiler_params=pltpu.CompilerParams(vmem_limit_bytes=12 * 1024 * 1024),
    )(*landed)


def solution(mesh):
    in_specs = (
        P(("gr", "fs"), None),
        P(("gr", "fs"), None),
        P(("gr", "fs"), None),
        P(("gr", "fs")),
        P(None, ("gr", "fs"), "tp"),
        P(None, ("gr", "fs"), "tp"),
        P(None, ("gr", "fs"), "tp"),
    )
    out_specs = (
        P("fs", None, "tp"),
        P("fs", None, "tp"),
        P("fs", None, "tp"),
        P(("gr", "fs"), "tp"),
    )
    return jax.shard_map(local, mesh=mesh, in_specs=in_specs, out_specs=out_specs, check_vma=False)
```

time: 111 us -> 100 us (0.901); the launches traced: 109 us -> 100 us
  local copies, waits for them, and re-layouts: 5.63 us -> 0 us
  Pallas kernels: 103 us -> 99.5 us
    unnamed x10 -> x0, local copies, waits for them, and re-layouts: 5.63 us -> none
    pallas_call x1 -> x2, Pallas kernels: 103 us -> 99.5 us  [the longest x1 97.7 us: local(): pl.pallas_call(kernel, name='hand_over', out_shape=(rows, rows, rows, slo...]
where the time goes in v2:
time: 100 us
  Pallas kernels  99.5 us (100%)
    pallas_call x1, Pallas kernels, local(): pl.pallas_call(kernel, name='hand_over', out_shape=(rows, rows, rows, slo...  97.7 us

profile of v2, /device:TPU:4, one launch (start us, length us, event | category | flops | bytes accessed | tf_op | source)
XLA Modules:
  0.0 100.1 jit_solution(13716602735294536938)
XLA Ops:
  0.6 97.7 %hand_over.1 = (bf16[2048,256]{1,0:T(8,128)(2,1)S(1)}, bf16[2048,256]{1,0:T(8,128)(2,1)S(1)}, bf16[2048,256]{1,0:T(8,128)(2,1)S(1)}, bf16[1280,256]{1,0:T(8,128)(2,1)S(1)}, bf16[1280,256]{1,0:T(8,128)(2,1)S(1)}) custom-call(bf16[256,2048]{1,0:T(8,128)(2,1)} %tok_h.1, s32[4,256]{1,0:T(4,128)} %bitcast.3, f32[4,256]{1,0:T(4,128)} %bitcast.4, f32[1,64]{1,0:T(1,128)} %bitcast.5, ...), custom_call_target="tpu_custom_call" | custom-call | tf_op jit(solution)/shard_map/hand_over/pallas_call | solution.py:383
  98.3 1.8 %write_out.1 = (bf16[1,2048,256]{2,1,0:T(8,128)(2,1)}, bf16[1,2048,256]{2,1,0:T(8,128)(2,1)}, bf16[1,2048,256]{2,1,0:T(8,128)(2,1)}, bf16[256,256]{1,0:T(8,128)(2,1)}) custom-call(bf16[2048,256]{1,0:T(8,128)(2,1)S(1)} %get-tuple-element.9.rcv1a, bf16[2048,256]{1,0:T(8,128)(2,1)S(1)} %get-tuple-element.10.rcv1b, ...), custom_call_target="tpu_custom_call" | custom-call | tf_op jit(solution)/shard_map/write_out/pallas_call | solution.py:423

commit v3 on v2

--- a/solution.py
+++ b/solution.py
@@ -28,6 +28,11 @@
 sigmoid_slope = 1.702
 
 
+SEQ = [7, 5, 6, 3, 4, 1, 2, 0]
+FIRST, LATER = SEQ[:EARLY], SEQ[EARLY:]
+ORDER = [(k, d) for d in (2, 1, 3, 0) for k in SEQ if k or d]
+
+
 def rem(a, n):
     return lax.rem(a, n)
 
@@ -38,17 +43,14 @@
     tok_v, ids_v, sc_v, gain_v, gate_v, up_v, down_v,
     qt, wt, onehot, normed, slots,
     wb1a, wb1b, wb2, ag1, ag2, acc, res,
-    load_sem, tok_send, tok_recv, w_send, w1a_recv, w1b_recv, w2_recv,
-    ag_send, ag1_recv, ag2a_recv, ag2b_recv, ret_send, ret_recv,
+    load_sem, tok_send, tok_recv, w_send, w_recv,
+    ag_send, ag1_recv, ag2a_recv, ag2b_recv, sib_recv, ret_send, ret_recv,
 ):
     gr, fs, tp = lax.axis_index("gr"), lax.axis_index("fs"), lax.axis_index("tp")
     z, y = gr * 4 + fs // 4, rem(fs, 4)
     x, core = tp // 2, rem(tp, 2)
     me = z * YS + y
 
-    def at(zz, yy):
-        return (zz // 4, rem(zz, 4) * 4 + yy, tp)
-
     def along(xx, cc):
         return (gr, fs, xx * 2 + cc)
 
@@ -63,6 +65,20 @@
 
     def landed(ref, sem):
         pltpu.make_async_copy(ref, ref, sem).wait()
+
+    planes = [rem(z + (away % ZS), ZS) for away in (0, 1, -1, 2, -2, 3, -3, 4)]
+    plane_gr, plane_fs = [p // 4 for p in planes], [rem(p, 4) * 4 for p in planes]
+    row = [y] + [rem(y + d, YS) for d in range(1, YS)]
+    peers = [(k, d) for k in range(ZS) for d in range(YS)][1:]
+
+    def peer(k, d):
+        return (plane_gr[k], plane_fs[k] + row[d], tp)
+
+    barrier = pltpu.get_barrier_semaphore()
+    for k, d in peers[::-1]:
+        pl.semaphore_signal(barrier, inc=1, device_id=peer(k, d), device_id_type=MESH)
+    for d in (right, left, sib):
+        pl.semaphore_signal(barrier, inc=1, device_id=d, device_id_type=MESH)
 
     loads = [
         pltpu.make_async_copy(s, d, load_sem.at[i])
@@ -73,17 +89,6 @@
     ]
     for c in loads:
         c.start()
-
-    barrier = pltpu.get_barrier_semaphore()
-
-    def greet(i, carry):
-        zz, yy = rem(z + i // 4, ZS), rem(y + rem(i, 4), YS)
-        pl.semaphore_signal(barrier, inc=1, device_id=at(zz, yy), device_id_type=MESH)
-        return carry
-
-    lax.fori_loop(1, ZS * YS, greet, 0)
-    for d in (right, left, sib):
-        pl.semaphore_signal(barrier, inc=1, device_id=d, device_id_type=MESH)
 
     loads[0].wait()
     loads[1].wait()
@@ -174,53 +179,34 @@
 
     pl.semaphore_wait(barrier, ZS * YS - 1 + 3)
 
-    def send_slots(zt, yt, group):
-        e = rem(zt, 4) * 4 + yt
-        remote(
-            slots.at[slot_rows(e)], ag1.at[tp, slot_rows(group * 4 + y)],
-            tok_send, tok_recv.at[group], at(zt, yt),
-        ).start()
-
-    def same_plane(i, carry):
-        send_slots(z, rem(y + i, YS), 3)
-        return carry
-
-    lax.fori_loop(1, YS, same_plane, 0)
-
-    def one_away(yt, carry):
-        send_slots(rem(z + 1, ZS), yt, 1)
-        send_slots(rem(z + 7, ZS), yt, 2)
-        return carry
-
-    lax.fori_loop(0, YS, one_away, 0)
-
-    def two_away(yt, carry):
-        step = jnp.where(rem(y + yt, 2) == 0, 2, 6)
-        send_slots(rem(z + step, ZS), yt, 0)
-        return carry
-
-    lax.fori_loop(0, YS, two_away, 0)
-
-    def plane(k):
-        away = (k + 1) // 2
-        return rem(z + jnp.where(rem(k, 2) == 1, away, ZS - away), ZS)
-
-    def send_weights(source, landing, send, recv):
-        def one(i, carry):
-            zt, yt = plane(i // 4), rem(y + rem(i, 4), YS)
+    def routes(group):
+        if group == 3:
+            return [(0, d) for d in range(1, YS)]
+        if group == 0:
+            return [(3 + d % 2, d) for d in range(YS)]
+        return [(group, d) for d in range(YS)]
+
+    for group in (3, 1, 2, 0):
+        for k, d in routes(group):
             remote(
-                source.at[rem(zt, 4) * 4 + yt], landing.at[own_rows],
-                send, recv.at[z], at(zt, yt),
+                slots.at[slot_rows(plane_fs[k] + row[d])], ag1.at[tp, slot_rows(group * 4 + y)],
+                tok_send, tok_recv.at[group], peer(k, d),
             ).start()
-            return carry
-
-        lax.fori_loop(1, ZS * YS, one, 0)
-
-    send_weights(wb1a, rcv1a, w_send.at[0], w1a_recv)
-    send_weights(wb1b, rcv1b, w_send.at[1], w1b_recv)
-    send_weights(wb2, rcv2, w_send.at[2], w2_recv)
-
-    def gather(buf, columns, send, recv):
+
+    def send_weights(source, landing, columns, send, recv):
+        for k, d in ORDER:
+            remote(
+                source.at[plane_fs[k] + row[d], :, columns], landing.at[own_rows, columns],
+                send, recv(k), peer(k, d),
+            ).start()
+
+    whole, low, high = pl.ds(0, COLS), pl.ds(0, SIDE), pl.ds(SIDE, SIDE)
+    send_weights(wb1a, rcv1a, whole, w_send.at[0], lambda k: w_recv.at[0])
+    send_weights(wb1b, rcv1b, whole, w_send.at[1], lambda k: w_recv.at[1])
+    send_weights(wb2, rcv2, low, w_send.at[2], lambda k: w_recv.at[2])
+    send_weights(wb2, rcv2, high, w_send.at[3], lambda k: w_recv.at[3 if k in FIRST else 4])
+
+    def gather(buf, columns, send, recv, sib_recv):
         def piece(xx, cc, start, size):
             return buf.at[xx * 2 + cc, pl.ds(start, size), columns]
 
@@ -228,29 +214,24 @@
             mine = piece(x, core, q * CHUNK, CHUNK)
             remote(mine, mine, send, recv.at[0, q], right).start()
             remote(mine, mine, send, recv.at[1, q], left).start()
-            remote(mine, mine, send, recv.at[4, q], sib).start()
+            remote(mine, mine, send, sib_recv, sib).start()
 
         def forward(q):
             whole = piece(x_left, core, q * CHUNK, CHUNK)
             landed(whole, recv.at[0, q])
             first = piece(x_left, core, q * CHUNK, HALF)
             remote(first, first, send, recv.at[2, q], right).start()
-            remote(whole, whole, send, recv.at[5, q], sib).start()
+            remote(whole, whole, send, sib_recv, sib).start()
             whole = piece(x_right, core, q * CHUNK, CHUNK)
             landed(whole, recv.at[1, q])
             second = piece(x_right, core, q * CHUNK + HALF, HALF)
-            remote(second, second, send, recv.at[3, q], left).start()
-            remote(whole, whole, send, recv.at[6, q], sib).start()
+            remote(second, second, send, recv.at[2, q], left).start()
+            remote(whole, whole, send, sib_recv, sib).start()
 
         def far(q):
-            landed(piece(x_far, core, q * CHUNK, HALF), recv.at[2, q])
-            landed(piece(x_far, core, q * CHUNK + HALF, HALF), recv.at[3, q])
-            whole = piece(x_far, core, q * CHUNK, CHUNK)
-            remote(whole, whole, send, recv.at[7, q], sib).start()
-
-        def others(q):
-            for i, xx in ((4, x), (5, x_left), (6, x_right), (7, x_far)):
-                landed(piece(xx, 1 - core, q * CHUNK, CHUNK), recv.at[i, q])
+            both = piece(x_far, core, q * CHUNK, CHUNK)
+            landed(both, recv.at[2, q])
+            remote(both, both, send, sib_recv, sib).start()
 
         def run(order, prepare):
             for i in range(CHUNKS + 3):
@@ -262,95 +243,82 @@
                 if 0 <= i - 4:
                     far(order[i - 4])
             far(order[CHUNKS - 1])
-            for q in range(CHUNKS):
-                others(q)
+            landed(buf.at[pl.ds(0, 4), :, columns], sib_recv)
 
         return run
 
     def group_landed(q):
         landed(ag1.at[0, pl.ds(0, (3 if q == 3 else 4) * CAP)], tok_recv.at[q])
 
-    gather(ag1, pl.ds(0, COLS), ag_send.at[0], ag1_recv)((3, 1, 2, 0), group_landed)
-
-    def planes_landed(landing, recv, first, end):
-        if first == 0:
-            landed(landing.at[pl.ds(0, 3 * OWN)], recv.at[z])
-
-        def one(k, carry):
-            landed(landing.at[pl.ds(0, 4 * OWN)], recv.at[plane(k)])
-            return carry
-
-        lax.fori_loop(max(first, 1), end, one, 0)
-
-    def product(left_of, right_of, rows, ks):
+    gather(ag1, whole, ag_send.at[0], ag1_recv, sib_recv.at[0])((3, 1, 2, 0), group_landed)
+
+    def product(left_of, right_of, rows, columns, ks):
         total = None
         for k in ks:
-            j = plane(k) if isinstance(ks, tuple) else k
+            j = planes[k] if isinstance(ks, tuple) else k
             start = pl.multiple_of(j * COLS, COLS) if isinstance(ks, tuple) else k * COLS
             part = jnp.dot(
-                left_of[j, rows, :], right_of[pl.ds(start, COLS), :], preferred_element_type=F32
+                left_of[j, rows, :], right_of[pl.ds(start, COLS), columns],
+                preferred_element_type=F32,
             )
             total = part if total is None else total + part
         return total
 
-    def half(landing, side, send, recv, hidden_recv):
-        columns = pl.ds(side * SIDE, SIDE)
-
+    def half(landing, side, columns, hidden_recv):
         def hidden(q):
             rows = pl.ds(q * CHUNK, CHUNK)
-            pre = product(ag1, landing, rows, range(ZS))
+            pre = product(ag1, landing, rows, whole, range(ZS))
             g = jnp.minimum(pre[:, :SIDE], clamp_limit)
             v = jnp.clip(pre[:, SIDE:], -clamp_limit, clamp_limit)
             ag2[tp, rows, columns] = (g * jax.nn.sigmoid(sigmoid_slope * g) * (v + 1.0)).astype(BF16)
 
-        planes_landed(landing, recv, 0, ZS)
-        gather(ag2, columns, send, hidden_recv)(tuple(range(CHUNKS)), hidden)
-
-    half(rcv1a, 0, ag_send.at[1], w1a_recv, ag2a_recv)
-    half(rcv1b, 1, ag_send.at[2], w1b_recv, ag2b_recv)
-
-    def send_back(group, ys, zs):
-        remote(
-            res.at[slot_rows(group * 4 + ys)], ret.at[slot_rows(fs)],
-            ret_send, ret_recv, at(zs, ys),
-        ).start()
-
-    def back(group):
-        def one(i, carry):
-            if group == 0:
-                step = jnp.where(rem(y + i, 2) == 0, 6, 2)
-                send_back(0, i, rem(z + step, ZS))
-            elif group < 3:
-                send_back(group, i, rem(z + (7 if group == 1 else 1), ZS))
-            else:
-                send_back(3, rem(y + i, YS), z)
-            return carry
-
-        lax.fori_loop(1 if group == 3 else 0, YS, one, 0)
-
-    planes_landed(rcv2, w2_recv, 0, EARLY)
+        landed(landing.at[pl.ds(0, 31 * OWN)], w_recv.at[side])
+        gather(ag2, columns, ag_send.at[1 + side], hidden_recv, sib_recv.at[1 + side])(
+            tuple(range(CHUNKS)), hidden
+        )
+
+    half(rcv1a, 0, low, ag2a_recv)
+    half(rcv1b, 1, high, ag2b_recv)
+
+    def back(group, side, columns):
+        for k, d in routes(group):
+            away = (0, 2, 1, 4, 3)[k]
+            remote(
+                res.at[slot_rows(group * 4 + row[d]), columns], ret.at[slot_rows(fs), columns],
+                ret_send.at[side], ret_recv.at[side], peer(away, d),
+            ).start()
+
+    landed(rcv2.at[pl.ds(0, 31 * OWN), low], w_recv.at[2])
+    for r in range(CHUNKS):
+        rows = pl.ds(r * CHUNK, CHUNK)
+        res[rows, low] = product(ag2, rcv2, rows, low, range(ZS)).astype(BF16)
+        back(r, 0, low)
+
+    landed(rcv2.at[pl.ds(0, (4 * EARLY - (0 in FIRST)) * OWN), high], w_recv.at[3])
 
     def begin(r, carry):
         rows = pl.ds(pl.multiple_of(r * CHUNK, CHUNK), CHUNK)
-        acc[rows, :] = product(ag2, rcv2, rows, tuple(range(EARLY)))
+        acc[rows, :] = product(ag2, rcv2, rows, high, tuple(FIRST))
         return carry
 
     lax.fori_loop(0, CHUNKS, begin, 0)
-    planes_landed(rcv2, w2_recv, EARLY, ZS)
+    landed(rcv2.at[pl.ds(0, (4 * (ZS - EARLY) - (0 in LATER)) * OWN), high], w_recv.at[4])
     for r in range(CHUNKS):
         rows = pl.ds(r * CHUNK, CHUNK)
-        res[rows, :] = (acc[rows, :] + product(ag2, rcv2, rows, tuple(range(EARLY, ZS)))).astype(BF16)
-        back(r)
+        late = product(ag2, rcv2, rows, high, tuple(LATER))
+        res[rows, high] = (acc[rows, :] + late).astype(BF16)
+        back(r, 1, high)
     ret[slot_rows(fs), :] = res[slot_rows(self_slot), :]
 
-    landed(ret.at[pl.ds(0, SLOTS - CAP)], ret_recv)
     landed(slots.at[pl.ds(0, SLOTS - CAP)], tok_send)
-    landed(ret.at[pl.ds(0, SLOTS - CAP)], ret_send)
-    for i, landing in enumerate((rcv1a, rcv1b, rcv2)):
+    for i, landing in enumerate((rcv1a, rcv1b, rcv2.at[:, low], rcv2.at[:, high])):
         landed(landing.at[pl.ds(0, 31 * OWN)], w_send.at[i])
     landed(ag1.at[pl.ds(0, 7)], ag_send.at[0])
-    landed(ag2.at[pl.ds(0, 7), :, pl.ds(0, SIDE)], ag_send.at[1])
-    landed(ag2.at[pl.ds(0, 7), :, pl.ds(0, SIDE)], ag_send.at[2])
+    for side in range(2):
+        landed(ag2.at[pl.ds(0, 7), :, pl.ds(0, SIDE)], ag_send.at[1 + side])
+        landed(ret.at[pl.ds(0, SLOTS - CAP), pl.ds(0, SIDE)], ret_send.at[side])
+    for side in range(2):
+        landed(ret.at[pl.ds(0, SLOTS - CAP), pl.ds(side * SIDE, SIDE)], ret_recv.at[side])
 
 
 def write_out(rcv1a, rcv1b, rcv2, ret, combine_t, og, ou, od, om, mix_v, sem):
@@ -404,13 +372,14 @@
             pltpu.VMEM((EXPERTS, OWN, COLS), BF16),
             pltpu.VMEM((TPS, SLOTS, COLS), BF16),
             pltpu.VMEM((TPS, SLOTS, COLS), BF16),
-            pltpu.VMEM((SLOTS, COLS), F32),
+            pltpu.VMEM((SLOTS, SIDE), F32),
             pltpu.VMEM((SLOTS, COLS), BF16),
-            dma((7,)), dma(()), dma((4,)), dma((3,)), dma((ZS,)), dma((ZS,)), dma((ZS,)),
-            dma((3,)), dma((8, CHUNKS)), dma((8, CHUNKS)), dma((8, CHUNKS)), dma(()), dma(()),
+            dma((7,)), dma(()), dma((4,)), dma((4,)), dma((5,)),
+            dma((3,)), dma((3, CHUNKS)), dma((3, CHUNKS)), dma((3, CHUNKS)), dma((3,)),
+            dma((2,)), dma((2,)),
         ],
         compiler_params=pltpu.CompilerParams(
-            collective_id=0, has_side_effects=True, vmem_limit_bytes=52 * 1000 * 1000
+            collective_id=0, has_side_effects=True, vmem_limit_bytes=44 * 1024 * 1024
         ),
     )(
         *(

time: 100 us -> 98.5 us (0.985)
  Pallas kernels: 99.5 us -> 97.8 us
    pallas_call x1, Pallas kernels: 97.7 us -> 96 us  [local(): pl.pallas_call(kernel, name='hand_over', out_shape=(rows, rows, rows, slo...]
where the time goes in v3:
time: 98.5 us; the launch traced here: 98.4 us
  Pallas kernels  97.8 us (99%)
    pallas_call x1, Pallas kernels, local(): pl.pallas_call(kernel, name='hand_over', out_shape=(rows, rows, rows, slo...  96 us

profile of v3, /device:TPU:4, one launch (start us, length us, event | category | flops | bytes accessed | tf_op | source)
XLA Modules:
  0.0 98.4 jit_solution(11174556405258559569)
XLA Ops:
  0.6 96.0 %hand_over.1 = (bf16[2048,256]{1,0:T(8,128)(2,1)S(1)}, bf16[2048,256]{1,0:T(8,128)(2,1)S(1)}, bf16[2048,256]{1,0:T(8,128)(2,1)S(1)}, bf16[1280,256]{1,0:T(8,128)(2,1)S(1)}, bf16[1280,256]{1,0:T(8,128)(2,1)S(1)}) custom-call(bf16[256,2048]{1,0:T(8,128)(2,1)} %tok_h.1, s32[4,256]{1,0:T(4,128)} %bitcast.3, f32[4,256]{1,0:T(4,128)} %bitcast.4, f32[1,64]{1,0:T(1,128)} %bitcast.5, ...), custom_call_target="tpu_custom_call" | custom-call | tf_op jit(solution)/shard_map/hand_over/pallas_call | solution.py:351
  96.6 1.8 %write_out.1 = (bf16[1,2048,256]{2,1,0:T(8,128)(2,1)}, bf16[1,2048,256]{2,1,0:T(8,128)(2,1)}, bf16[1,2048,256]{2,1,0:T(8,128)(2,1)}, bf16[256,256]{1,0:T(8,128)(2,1)}) custom-call(bf16[2048,256]{1,0:T(8,128)(2,1)S(1)} %get-tuple-element.9.rcv1a, bf16[2048,256]{1,0:T(8,128)(2,1)S(1)} %get-tuple-element.10.rcv1b, ...), custom_call_target="tpu_custom_call" | custom-call | tf_op jit(solution)/shard_map/write_out/pallas_call | solution.py:392

commit v4 on v3

--- a/solution.py
+++ b/solution.py
@@ -21,6 +21,7 @@
 CHUNKS = 4
 CHUNK = SLOTS // CHUNKS
 HALF = CHUNK // 2
+AHEAD = 6
 EARLY = 5
 
 norm_eps = 1e-06
@@ -41,9 +42,9 @@
     tok_h, ids_h, sc_h, gain_h, gate_h, up_h, down_h,
     rcv1a, rcv1b, rcv2, ret, combine_t,
     tok_v, ids_v, sc_v, gain_v, gate_v, up_v, down_v,
-    qt, wt, onehot, normed, slots,
+    qt, wt, onehot, normed, slots, rows_in, ids_in,
     wb1a, wb1b, wb2, ag1, ag2, acc, res,
-    load_sem, tok_send, tok_recv, w_send, w_recv,
+    load_sem, near_send, near_recv, tok_send, tok_recv, w_send, w_recv,
     ag_send, ag1_recv, ag2a_recv, ag2b_recv, sib_recv, ret_send, ret_recv,
 ):
     gr, fs, tp = lax.axis_index("gr"), lax.axis_index("fs"), lax.axis_index("tp")
@@ -90,38 +91,31 @@
     for c in loads:
         c.start()
 
-    loads[0].wait()
-    loads[1].wait()
-    ids = ids_v[...]
-    exponent = jnp.exp(sc_v[...])
-    total = jnp.sum(exponent, axis=0, keepdims=True)
-    weights = (exponent / total).astype(BF16).astype(F32)
     expert_of = lax.broadcasted_iota(jnp.int32, (EXPERTS, ROWS), 0)
-    member = jnp.zeros((EXPERTS, ROWS), F32)
-    weight_of = jnp.zeros((EXPERTS, ROWS), F32)
-    for k in range(TOP):
-        same = ids[k : k + 1, :] == expert_of
-        member = member + jnp.where(same, 1.0, 0.0)
-        weight_of = weight_of + jnp.where(same, weights[k : k + 1, :], 0.0)
     earlier = jnp.where(
         lax.broadcasted_iota(jnp.int32, (ROWS, ROWS), 0)
         < lax.broadcasted_iota(jnp.int32, (ROWS, ROWS), 1),
         1.0, 0.0,
     ).astype(BF16)
-    before = jnp.dot(member.astype(BF16), earlier, preferred_element_type=F32)
-    qt[...] = jnp.where(member > 0.5, before, -1.0)
-    wt[...] = weight_of
+
+    def slot_table(ids):
+        member = jnp.zeros((EXPERTS, ROWS), F32)
+        for k in range(TOP):
+            member = member + jnp.where(ids[k : k + 1, :] == expert_of, 1.0, 0.0)
+        before = jnp.dot(member.astype(BF16), earlier, preferred_element_type=F32)
+        return jnp.where(member > 0.5, before, -1.0)
 
     slot_no = lax.broadcasted_iota(jnp.int32, (CAP, ROWS), 0).astype(F32)
 
-    def tables(e, carry):
-        hit = qt[pl.ds(e, 1), :] == slot_no
-        rows = pl.ds(pl.multiple_of(e * CAP, 16), CAP)
-        onehot[rows, :] = jnp.where(hit, 1.0, 0.0).astype(BF16)
-        combine_t[rows, :] = jnp.where(hit, wt[pl.ds(e, 1), :], 0.0).astype(BF16)
-        return carry
-
-    lax.fori_loop(0, EXPERTS, tables, 0)
+    def fill(table, rows, experts, out):
+        for i, e in enumerate(experts):
+            hit = qt[table, pl.ds(e, 1), :] == slot_no
+            onehot[i * CAP : (i + 1) * CAP, :] = jnp.where(hit, 1.0, 0.0).astype(BF16)
+        n = len(experts) * CAP
+        out[0:n, :] = jnp.dot(onehot[0:n, :], rows, preferred_element_type=F32).astype(BF16)
+
+    loads[0].wait()
+    qt[0] = slot_table(ids_v[...])
 
     loads[2].wait()
 
@@ -135,14 +129,9 @@
 
     lax.fori_loop(0, ROWS // 32, norm, 0)
 
-    def fill(i, carry):
-        rows = pl.ds(pl.multiple_of(i * CHUNK, CHUNK), CHUNK)
-        slots[rows, :] = jnp.dot(
-            onehot[rows, :], normed[...], preferred_element_type=F32
-        ).astype(BF16)
-        return carry
-
-    lax.fori_loop(0, CHUNKS, fill, 0)
+    here = [plane_fs[0] + row[d] for d in range(YS)]
+    slots_own = slots.at[0]
+    fill(0, normed[...], here, slots_own)
 
     loads[3].wait()
     square = (OWN, OWN)
@@ -175,7 +164,7 @@
         return pl.ds(pl.multiple_of(e * CAP, 16), CAP)
 
     self_slot = 3 * 4 + y
-    ag1[tp, slot_rows(self_slot), :] = slots[slot_rows(fs), :]
+    ag1[tp, slot_rows(self_slot), :] = slots_own[0:CAP, :]
 
     pl.semaphore_wait(barrier, ZS * YS - 1 + 3)
 
@@ -186,22 +175,61 @@
             return [(3 + d % 2, d) for d in range(YS)]
         return [(group, d) for d in range(YS)]
 
-    for group in (3, 1, 2, 0):
-        for k, d in routes(group):
-            remote(
-                slots.at[slot_rows(plane_fs[k] + row[d])], ag1.at[tp, slot_rows(group * 4 + y)],
-                tok_send, tok_recv.at[group], peer(k, d),
-            ).start()
-
-    def send_weights(source, landing, columns, send, recv):
-        for k, d in ORDER:
+    up, below = peer(1, 0), peer(2, 0)
+    for side, device in enumerate((up, below)):
+        remote(normed, rows_in.at[side], near_send.at[0], near_recv.at[side], device).start()
+        remote(ids_v, ids_in.at[side], near_send.at[1], near_recv.at[2 + side], device).start()
+
+    def send_slots(side, i, group, k, d):
+        remote(
+            slots.at[side, pl.ds(i * CAP, CAP)], ag1.at[tp, slot_rows(group * 4 + y)],
+            tok_send, tok_recv.at[group], peer(k, d),
+        ).start()
+
+    for d in range(1, YS):
+        send_slots(0, d, 3, 0, d)
+
+    def send_weights(source, landing, columns, send, recv, some=slice(None)):
+        for k, d in ORDER[some]:
             remote(
                 source.at[plane_fs[k] + row[d], :, columns], landing.at[own_rows, columns],
                 send, recv(k), peer(k, d),
             ).start()
 
     whole, low, high = pl.ds(0, COLS), pl.ds(0, SIDE), pl.ds(SIDE, SIDE)
-    send_weights(wb1a, rcv1a, whole, w_send.at[0], lambda k: w_recv.at[0])
+    send_weights(wb1a, rcv1a, whole, w_send.at[0], lambda k: w_recv.at[0], slice(0, AHEAD))
+
+    loads[1].wait()
+    ids, exponent = ids_v[...], jnp.exp(sc_v[...])
+    total = jnp.sum(exponent, axis=0, keepdims=True)
+    weights = (exponent / total).astype(BF16).astype(F32)
+    weight_of = jnp.zeros((EXPERTS, ROWS), F32)
+    for k in range(TOP):
+        weight_of = weight_of + jnp.where(ids[k : k + 1, :] == expert_of, weights[k : k + 1, :], 0.0)
+    wt[...] = weight_of
+
+    def combine(e, carry):
+        hit = qt[0, pl.ds(e, 1), :] == slot_no
+        rows = pl.ds(pl.multiple_of(e * CAP, 16), CAP)
+        combine_t[rows, :] = jnp.where(hit, wt[pl.ds(e, 1), :], 0.0).astype(BF16)
+        return carry
+
+    lax.fori_loop(0, EXPERTS, combine, 0)
+
+    for side in range(2):
+        landed(ids_in.at[side], near_recv.at[2 + side])
+        landed(rows_in.at[side], near_recv.at[side])
+        qt[1 + side] = slot_table(ids_in[side])
+        beyond = [(1 + side, d) for d in range(side, YS, 2)]
+        experts = here + [plane_fs[k] + row[d] for k, d in beyond]
+        fill(1 + side, rows_in[side], experts, slots.at[1 + side])
+        for i, (k, d) in enumerate(beyond):
+            send_slots(1 + side, YS + i, 0, k, d)
+        for d in range(1, YS):
+            send_slots(1 + side, d, 1 + side, 0, d)
+        ag1[tp, slot_rows((1 + side) * 4 + y), :] = slots[1 + side, 0:CAP, :]
+
+    send_weights(wb1a, rcv1a, whole, w_send.at[0], lambda k: w_recv.at[0], slice(AHEAD, None))
     send_weights(wb1b, rcv1b, whole, w_send.at[1], lambda k: w_recv.at[1])
     send_weights(wb2, rcv2, low, w_send.at[2], lambda k: w_recv.at[2])
     send_weights(wb2, rcv2, high, w_send.at[3], lambda k: w_recv.at[3 if k in FIRST else 4])
@@ -248,7 +276,7 @@
         return run
 
     def group_landed(q):
-        landed(ag1.at[0, pl.ds(0, (3 if q == 3 else 4) * CAP)], tok_recv.at[q])
+        landed(ag1.at[0, pl.ds(0, (4 if q == 0 else 3) * CAP)], tok_recv.at[q])
 
     gather(ag1, whole, ag_send.at[0], ag1_recv, sib_recv.at[0])((3, 1, 2, 0), group_landed)
 
@@ -310,7 +338,9 @@
         back(r, 1, high)
     ret[slot_rows(fs), :] = res[slot_rows(self_slot), :]
 
-    landed(slots.at[pl.ds(0, SLOTS - CAP)], tok_send)
+    landed(ret.at[pl.ds(0, 13 * CAP)], tok_send)
+    landed(rows_in, near_send.at[0])
+    landed(ids_in, near_send.at[1])
     for i, landing in enumerate((rcv1a, rcv1b, rcv2.at[:, low], rcv2.at[:, high])):
         landed(landing.at[pl.ds(0, 31 * OWN)], w_send.at[i])
     landed(ag1.at[pl.ds(0, 7)], ag_send.at[0])
@@ -362,11 +392,13 @@
             pltpu.VMEM((EXPERTS, OWN, COLS), F32),
             pltpu.VMEM((EXPERTS, OWN, COLS), F32),
             pltpu.VMEM((EXPERTS, OWN, COLS), F32),
+            pltpu.VMEM((3, EXPERTS, ROWS), F32),
             pltpu.VMEM((EXPERTS, ROWS), F32),
-            pltpu.VMEM((EXPERTS, ROWS), F32),
-            pltpu.VMEM((SLOTS, ROWS), BF16),
+            pltpu.VMEM((6 * CAP, ROWS), BF16),
             pltpu.VMEM((ROWS, COLS), BF16),
-            pltpu.VMEM((SLOTS, COLS), BF16),
+            pltpu.VMEM((3, 6 * CAP, COLS), BF16),
+            pltpu.VMEM((2, ROWS, COLS), BF16),
+            pltpu.VMEM((2, TOP, ROWS), jnp.int32),
             pltpu.VMEM((EXPERTS, OWN, COLS), BF16),
             pltpu.VMEM((EXPERTS, OWN, COLS), BF16),
             pltpu.VMEM((EXPERTS, OWN, COLS), BF16),
@@ -374,7 +406,7 @@
             pltpu.VMEM((TPS, SLOTS, COLS), BF16),
             pltpu.VMEM((SLOTS, SIDE), F32),
             pltpu.VMEM((SLOTS, COLS), BF16),
-            dma((7,)), dma(()), dma((4,)), dma((4,)), dma((5,)),
+            dma((7,)), dma((2,)), dma((4,)), dma(()), dma((4,)), dma((4,)), dma((5,)),
             dma((3,)), dma((3, CHUNKS)), dma((3, CHUNKS)), dma((3, CHUNKS)), dma((3,)),
             dma((2,)), dma((2,)),
         ],

time: 98.5 us -> 95.7 us (0.972)
  Pallas kernels: 97.8 us -> 94.9 us
    pallas_call x1, Pallas kernels: 96 us -> 93.1 us  [local(): pl.pallas_call(kernel, name='hand_over', out_shape=(rows, rows, rows, slo...]
where the time goes in v4:
time: 95.7 us; the launch traced here: 95.5 us
  Pallas kernels  94.9 us (99%)
    pallas_call x1, Pallas kernels, local(): pl.pallas_call(kernel, name='hand_over', out_shape=(rows, rows, rows, slo...  93.1 us

profile of v4, /device:TPU:4, one launch (start us, length us, event | category | flops | bytes accessed | tf_op | source)
XLA Modules:
  0.0 95.5 jit_solution(15212244796770271634)
XLA Ops:
  0.6 93.1 %hand_over.1 = (bf16[2048,256]{1,0:T(8,128)(2,1)S(1)}, bf16[2048,256]{1,0:T(8,128)(2,1)S(1)}, bf16[2048,256]{1,0:T(8,128)(2,1)S(1)}, bf16[1280,256]{1,0:T(8,128)(2,1)S(1)}, bf16[1280,256]{1,0:T(8,128)(2,1)S(1)}) custom-call(bf16[256,2048]{1,0:T(8,128)(2,1)} %tok_h.1, s32[4,256]{1,0:T(4,128)} %bitcast.3, f32[4,256]{1,0:T(4,128)} %bitcast.4, f32[1,64]{1,0:T(1,128)} %bitcast.5, ...), custom_call_target="tpu_custom_call" | custom-call | tf_op jit(solution)/shard_map/hand_over/pallas_call | solution.py:381
  93.8 1.8 %write_out.1 = (bf16[1,2048,256]{2,1,0:T(8,128)(2,1)}, bf16[1,2048,256]{2,1,0:T(8,128)(2,1)}, bf16[1,2048,256]{2,1,0:T(8,128)(2,1)}, bf16[256,256]{1,0:T(8,128)(2,1)}) custom-call(bf16[2048,256]{1,0:T(8,128)(2,1)S(1)} %get-tuple-element.9.rcv1a, bf16[2048,256]{1,0:T(8,128)(2,1)S(1)} %get-tuple-element.10.rcv1b, ...), custom_call_target="tpu_custom_call" | custom-call | tf_op jit(solution)/shard_map/write_out/pallas_call | solution.py:424

commit v5 on v4

--- a/solution.py
+++ b/solution.py
@@ -22,7 +22,6 @@
 CHUNK = SLOTS // CHUNKS
 HALF = CHUNK // 2
 AHEAD = 6
-EARLY = 5
 
 norm_eps = 1e-06
 clamp_limit = 7.0
@@ -30,8 +29,9 @@
 
 
 SEQ = [7, 5, 6, 3, 4, 1, 2, 0]
-FIRST, LATER = SEQ[:EARLY], SEQ[EARLY:]
+FIRST, LATER = [7, 5, 6, 3, 4], [1, 2, 0]
 ORDER = [(k, d) for d in (2, 1, 3, 0) for k in SEQ if k or d]
+LAST_ORDER = [(k, d) for k in FIRST + LATER for d in (2, 1, 3, 0) if k or d]
 
 
 def rem(a, n):
@@ -129,6 +129,13 @@
 
     lax.fori_loop(0, ROWS // 32, norm, 0)
 
+    pl.semaphore_wait(barrier, ZS * YS - 1 + 3)
+
+    up, below = peer(1, 0), peer(2, 0)
+    for side, device in enumerate((up, below)):
+        remote(normed, rows_in.at[side], near_send.at[0], near_recv.at[side], device).start()
+        remote(ids_v, ids_in.at[side], near_send.at[1], near_recv.at[2 + side], device).start()
+
     here = [plane_fs[0] + row[d] for d in range(YS)]
     slots_own = slots.at[0]
     fill(0, normed[...], here, slots_own)
@@ -166,8 +173,6 @@
     self_slot = 3 * 4 + y
     ag1[tp, slot_rows(self_slot), :] = slots_own[0:CAP, :]
 
-    pl.semaphore_wait(barrier, ZS * YS - 1 + 3)
-
     def routes(group):
         if group == 3:
             return [(0, d) for d in range(1, YS)]
@@ -175,11 +180,6 @@
             return [(3 + d % 2, d) for d in range(YS)]
         return [(group, d) for d in range(YS)]
 
-    up, below = peer(1, 0), peer(2, 0)
-    for side, device in enumerate((up, below)):
-        remote(normed, rows_in.at[side], near_send.at[0], near_recv.at[side], device).start()
-        remote(ids_v, ids_in.at[side], near_send.at[1], near_recv.at[2 + side], device).start()
-
     def send_slots(side, i, group, k, d):
         remote(
             slots.at[side, pl.ds(i * CAP, CAP)], ag1.at[tp, slot_rows(group * 4 + y)],
@@ -189,15 +189,15 @@
     for d in range(1, YS):
         send_slots(0, d, 3, 0, d)
 
-    def send_weights(source, landing, columns, send, recv, some=slice(None)):
-        for k, d in ORDER[some]:
+    def send_weights(source, landing, columns, send, recv, order):
+        for k, d in order:
             remote(
                 source.at[plane_fs[k] + row[d], :, columns], landing.at[own_rows, columns],
                 send, recv(k), peer(k, d),
             ).start()
 
     whole, low, high = pl.ds(0, COLS), pl.ds(0, SIDE), pl.ds(SIDE, SIDE)
-    send_weights(wb1a, rcv1a, whole, w_send.at[0], lambda k: w_recv.at[0], slice(0, AHEAD))
+    send_weights(wb1a, rcv1a, whole, w_send.at[0], lambda k: w_recv.at[0], ORDER[:AHEAD])
 
     loads[1].wait()
     ids, exponent = ids_v[...], jnp.exp(sc_v[...])
@@ -229,10 +229,10 @@
             send_slots(1 + side, d, 1 + side, 0, d)
         ag1[tp, slot_rows((1 + side) * 4 + y), :] = slots[1 + side, 0:CAP, :]
 
-    send_weights(wb1a, rcv1a, whole, w_send.at[0], lambda k: w_recv.at[0], slice(AHEAD, None))
-    send_weights(wb1b, rcv1b, whole, w_send.at[1], lambda k: w_recv.at[1])
-    send_weights(wb2, rcv2, low, w_send.at[2], lambda k: w_recv.at[2])
-    send_weights(wb2, rcv2, high, w_send.at[3], lambda k: w_recv.at[3 if k in FIRST else 4])
+    send_weights(wb1a, rcv1a, whole, w_send.at[0], lambda k: w_recv.at[0], ORDER[AHEAD:])
+    send_weights(wb1b, rcv1b, whole, w_send.at[1], lambda k: w_recv.at[1], ORDER)
+    send_weights(wb2, rcv2, low, w_send.at[2], lambda k: w_recv.at[2], ORDER)
+    send_weights(wb2, rcv2, high, w_send.at[3], lambda k: w_recv.at[3 if k in FIRST else 4], LAST_ORDER)
 
     def gather(buf, columns, send, recv, sib_recv):
         def piece(xx, cc, start, size):
@@ -322,7 +322,7 @@
         res[rows, low] = product(ag2, rcv2, rows, low, range(ZS)).astype(BF16)
         back(r, 0, low)
 
-    landed(rcv2.at[pl.ds(0, (4 * EARLY - (0 in FIRST)) * OWN), high], w_recv.at[3])
+    landed(rcv2.at[pl.ds(0, (4 * len(FIRST) - (0 in FIRST)) * OWN), high], w_recv.at[3])
 
     def begin(r, carry):
         rows = pl.ds(pl.multiple_of(r * CHUNK, CHUNK), CHUNK)
@@ -330,7 +330,7 @@
         return carry
 
     lax.fori_loop(0, CHUNKS, begin, 0)
-    landed(rcv2.at[pl.ds(0, (4 * (ZS - EARLY) - (0 in LATER)) * OWN), high], w_recv.at[4])
+    landed(rcv2.at[pl.ds(0, (4 * len(LATER) - (0 in LATER)) * OWN), high], w_recv.at[4])
     for r in range(CHUNKS):
         rows = pl.ds(r * CHUNK, CHUNK)
         late = product(ag2, rcv2, rows, high, tuple(LATER))

time: 95.7 us -> 95.6 us (level)
  no operation moved by 1% of the time
where the time goes in v5:
time: 95.6 us; the launch traced here: 95.5 us
  Pallas kernels  94.9 us (99%)
    pallas_call x1, Pallas kernels, local(): pl.pallas_call(kernel, name='hand_over', out_shape=(rows, rows, rows, slo...  93.1 us

profile of v5, /device:TPU:4, one launch (start us, length us, event | category | flops | bytes accessed | tf_op | source)
XLA Modules:
  0.0 95.5 jit_solution(2829011548272504894)
XLA Ops:
  0.6 93.1 %hand_over.1 = (bf16[2048,256]{1,0:T(8,128)(2,1)S(1)}, bf16[2048,256]{1,0:T(8,128)(2,1)S(1)}, bf16[2048,256]{1,0:T(8,128)(2,1)S(1)}, bf16[1280,256]{1,0:T(8,128)(2,1)S(1)}, bf16[1280,256]{1,0:T(8,128)(2,1)S(1)}) custom-call(bf16[256,2048]{1,0:T(8,128)(2,1)} %tok_h.1, s32[4,256]{1,0:T(4,128)} %bitcast.3, f32[4,256]{1,0:T(4,128)} %bitcast.4, f32[1,64]{1,0:T(1,128)} %bitcast.5, ...), custom_call_target="tpu_custom_call" | custom-call | tf_op jit(solution)/shard_map/hand_over/pallas_call | solution.py:381
  93.8 1.8 %write_out.1 = (bf16[1,2048,256]{2,1,0:T(8,128)(2,1)}, bf16[1,2048,256]{2,1,0:T(8,128)(2,1)}, bf16[1,2048,256]{2,1,0:T(8,128)(2,1)}, bf16[256,256]{1,0:T(8,128)(2,1)}) custom-call(bf16[2048,256]{1,0:T(8,128)(2,1)S(1)} %get-tuple-element.9.rcv1a, bf16[2048,256]{1,0:T(8,128)(2,1)S(1)} %get-tuple-element.10.rcv1b, ...), custom_call_target="tpu_custom_call" | custom-call | tf_op jit(solution)/shard_map/write_out/pallas_call | solution.py:424

commit v6 on v5

--- a/solution.py
+++ b/solution.py
@@ -29,7 +29,7 @@
 
 
 SEQ = [7, 5, 6, 3, 4, 1, 2, 0]
-FIRST, LATER = [7, 5, 6, 3, 4], [1, 2, 0]
+FIRST, LATER = [0, 7, 5, 6, 3, 4], [1, 2]
 ORDER = [(k, d) for d in (2, 1, 3, 0) for k in SEQ if k or d]
 LAST_ORDER = [(k, d) for k in FIRST + LATER for d in (2, 1, 3, 0) if k or d]
 

time: 95.6 us -> 95.7 us (level)
  no operation moved by 1% of the time
where the time goes in v6:
time: 95.7 us; the launch traced here: 95.6 us
  Pallas kernels  95 us (99%)
    pallas_call x1, Pallas kernels, local(): pl.pallas_call(kernel, name='hand_over', out_shape=(rows, rows, rows, slo...  93.2 us

profile of v6, /device:TPU:4, one launch (start us, length us, event | category | flops | bytes accessed | tf_op | source)
XLA Modules:
  0.0 95.6 jit_solution(10316296615262859476)
XLA Ops:
  0.6 93.2 %hand_over.1 = (bf16[2048,256]{1,0:T(8,128)(2,1)S(1)}, bf16[2048,256]{1,0:T(8,128)(2,1)S(1)}, bf16[2048,256]{1,0:T(8,128)(2,1)S(1)}, bf16[1280,256]{1,0:T(8,128)(2,1)S(1)}, bf16[1280,256]{1,0:T(8,128)(2,1)S(1)}) custom-call(bf16[256,2048]{1,0:T(8,128)(2,1)} %tok_h.1, s32[4,256]{1,0:T(4,128)} %bitcast.3, f32[4,256]{1,0:T(4,128)} %bitcast.4, f32[1,64]{1,0:T(1,128)} %bitcast.5, ...), custom_call_target="tpu_custom_call" | custom-call | tf_op jit(solution)/shard_map/hand_over/pallas_call | solution.py:381
  93.8 1.8 %write_out.1 = (bf16[1,2048,256]{2,1,0:T(8,128)(2,1)}, bf16[1,2048,256]{2,1,0:T(8,128)(2,1)}, bf16[1,2048,256]{2,1,0:T(8,128)(2,1)}, bf16[256,256]{1,0:T(8,128)(2,1)}) custom-call(bf16[2048,256]{1,0:T(8,128)(2,1)S(1)} %get-tuple-element.9.rcv1a, bf16[2048,256]{1,0:T(8,128)(2,1)S(1)} %get-tuple-element.10.rcv1b, ...), custom_call_target="tpu_custom_call" | custom-call | tf_op jit(solution)/shard_map/write_out/pallas_call | solution.py:424
